TPU v7x, 128 devices: a whole 4x4x4 slice. The times are simulated.
128 devices in a mesh: sp: 16 (over z, y), tp: 8 (over x, core).
Axes of the slice: x: 4, y: 4, z: 4, core: 2. Of those that a mesh axis runs over, the one named last changes fastest.
Arguments:
- tokens: bfloat16 [32768, 2048], P('sp'), may hold values from -6 to 6
- w_query: bfloat16 [2048, 1024], P(None, 'tp'), may hold values from -0.125 to 0.125
- w_key: bfloat16 [2048, 1024], P(None, 'tp'), may hold values from -0.125 to 0.125
- w_value: bfloat16 [2048, 1024], P(None, 'tp'), may hold values from -0.125 to 0.125
- w_gate: bfloat16 [2048, 1024], P(None, 'tp'), may hold values from -0.125 to 0.125
- w_pool: bfloat16 [2048, 1024], P(None, 'tp'), may hold values from -0.125 to 0.125
- norm_gain: float32 [1024], P('tp'), may hold values from 0.1 to 1.9
- log_decay: float32 [8, 32768], P('tp', 'sp'), may hold values from -0.8 to 0
- w_out: bfloat16 [2048, 2048], replicated, may hold values from -0.125 to 0.125
Outputs:
- mixed_out: bfloat16 [32768, 2048], P(('sp', 'tp'))
All inputs are finite; a program needn't handle non-finite values.
Results may differ from a plain program's by a relative error of at most 0.014.
Values may be sent and summed in bfloat16 or wider, within the bound.
A program may use at most 64 MiB of HBM per device.

v0:
```python
import jax
import jax.numpy as jnp
from jax import lax
from jax.sharding import PartitionSpec as P

HEAD_DIM = 128
POOL_GROUP = 256
BLOCK = 128
RET_WIDTH = 1024


def passed_along(block, axis, distance):
    devices = range(lax.axis_size(axis))
    route = [(i - distance, i) for i in devices if i - distance in devices]
    return lax.ppermute(block, axis, route)


def from_everyone(array, axis):
    peers = lax.axis_size(axis)
    return lax.all_to_all(
        jnp.broadcast_to(array[None], (peers, *array.shape)), axis, 0, 0, tiled=True
    )


def collected_together(array, axis):
    leaves = jax.tree.leaves(array)
    order = sorted(range(len(leaves)), key=lambda k: -leaves[k].size)
    width = (1, *leaves[order[0]].shape)[-1]
    lines = [
        jnp.pad(leaves[k].reshape(-1), (0, -leaves[k].size % width)).reshape(-1, width)
        for k in order
    ]
    both, at, found = (from_everyone(jnp.concatenate(lines), axis), 0, {})
    for k, line in zip(order, lines):
        share = both[:, at : at + len(line)].reshape(len(both), -1)
        found[k] = share[:, : leaves[k].size].reshape(-1, *leaves[k].shape)
        at += len(line)
    numbers = iter(range(len(leaves)))
    return jax.tree.map(lambda _: found[next(numbers)], array)


def folded_in_pairs(pieces, combine):
    while len(jax.tree.leaves(pieces)[0]) > 1:
        pieces = jax.vmap(combine)(
            *(jax.tree.map(lambda part: part[side::2], pieces) for side in (0, 1))
        )
    return jax.tree.map(lambda part: part[0], pieces)


def carried_in(array, axis, combine, identity):
    peers, here = (lax.axis_size(axis), lax.axis_index(axis))
    passed = jnp.arange(peers) < here

    def kept(part, zero, own):
        part = jnp.where(
            passed.reshape(-1, *(1 for _ in own.shape)), part, jnp.asarray(zero, own.dtype)
        )
        return part

    pieces = collected_together(array, axis)
    return folded_in_pairs(jax.tree.map(kept, pieces, identity, array), combine)


def rotate(tensor, positions):
    half_dim = tensor.shape[-1] // 2
    inverse = 10000.0 ** (-jnp.arange(half_dim, dtype=jnp.float32) / half_dim)
    angles = positions.astype(jnp.float32)[:, None] * inverse[None, :]
    cosine = jnp.cos(angles)[:, None, :]
    sine_part = jnp.sin(angles)[:, None, :]
    first_half = tensor[..., :half_dim]
    second_half = tensor[..., half_dim:]
    return jnp.concatenate(
        [
            first_half * cosine - second_half * sine_part,
            first_half * sine_part + second_half * cosine,
        ],
        axis=-1,
    )


def block_parts(q_blocks, k_blocks, v_blocks, decay_blocks):
    log_cum = jnp.cumsum(decay_blocks, axis=1)
    block_ends = log_cum[:, -1, :]
    steps_len = q_blocks.shape[1]
    causal = jnp.arange(steps_len)[:, None] >= jnp.arange(steps_len)[None, :]
    head_cum = jnp.transpose(log_cum, (0, 2, 1))
    log_gap = head_cum[:, :, :, None] - head_cum[:, :, None, :]
    weights = jnp.where(causal[None, None], jnp.exp(jnp.minimum(log_gap, 0.0)), 0.0)
    scores = jnp.einsum("nthd,nshd->nhts", q_blocks, k_blocks, preferred_element_type=jnp.float32)
    mixing = (scores * weights).astype(jnp.bfloat16)
    inner_part = jnp.einsum("nhts,nshe->nthe", mixing, v_blocks, preferred_element_type=jnp.float32)
    keys_decayed = (
        k_blocks.astype(jnp.float32) * jnp.exp(block_ends[:, None, :] - log_cum)[..., None]
    ).astype(jnp.bfloat16)
    updates = jnp.einsum(
        "nshd,nshe->nhde", keys_decayed, v_blocks, preferred_element_type=jnp.float32
    )
    return (log_cum, block_ends, inner_part, updates)


def chain_states(earlier, later):
    return (earlier[0] * later[0], earlier[1] * later[0][:, None, None] + later[1])


def local(tokens, w_query, w_key, w_value, w_gate, w_pool, norm_gain, log_decay, w_out):
    tok_rows = tokens.shape[0]
    n_heads = w_query.shape[1] // HEAD_DIM
    seq_index = lax.axis_index("sp")
    head_index = lax.axis_index("tp")

    def project(weights):
        return jnp.dot(tokens, weights, preferred_element_type=jnp.float32).astype(jnp.bfloat16)

    query = project(w_query)
    keys_raw = project(w_key)
    values = project(w_value)
    gate_pre = project(w_gate)
    pool_in = project(w_pool)
    rim_rows = passed_along(pool_in[tok_rows - 15 :], "sp", 1)
    positions = seq_index * tok_rows + jnp.arange(tok_rows)
    head_shape = (tok_rows, n_heads, HEAD_DIM)
    q_rot = rotate(query.astype(jnp.float32).reshape(head_shape), positions).astype(jnp.bfloat16)
    k_rot = (
        rotate(keys_raw.astype(jnp.float32).reshape(head_shape), positions) * HEAD_DIM ** (-0.5)
    ).astype(jnp.bfloat16)
    n_blocks = tok_rows // BLOCK
    block_shape = (n_blocks, BLOCK, n_heads, HEAD_DIM)
    q_blocks = q_rot.reshape(block_shape)
    k_blocks = k_rot.reshape(block_shape)
    v_blocks = values.reshape(block_shape)
    decay_blocks = jnp.transpose(log_decay).reshape(n_blocks, BLOCK, n_heads)
    log_cum, block_ends, inner_part, updates = block_parts(
        q_blocks, k_blocks, v_blocks, decay_blocks
    )

    def advance(running, element):
        block_end, update_n = element
        return (running * jnp.exp(block_end)[:, None, None] + update_n, running)

    zero_state = jnp.zeros((n_heads, HEAD_DIM, HEAD_DIM), jnp.float32)
    final_local, before_local = lax.scan(advance, zero_state, (block_ends, updates))
    end_cum = jnp.cumsum(block_ends, axis=0)
    dev_total = jnp.exp(end_cum[-1])
    reach = jnp.exp(end_cum - block_ends)
    identity = (jnp.ones_like(dev_total), jnp.zeros_like(final_local))
    _, incoming = carried_in((dev_total, final_local), "sp", chain_states, identity)
    before_state = before_local + reach[:, :, None, None] * incoming[None]
    state_bf = before_state.astype(jnp.bfloat16)
    cross_part = (
        jnp.einsum("nthd,nhde->nthe", q_blocks, state_bf, preferred_element_type=jnp.float32)
        * jnp.exp(log_cum)[..., None]
    )
    retained = (inner_part + cross_part).reshape(head_shape)
    centered = retained - jnp.mean(retained, axis=-1, keepdims=True)
    normed = centered * lax.rsqrt(jnp.mean(centered * centered, axis=-1, keepdims=True) + 1e-06)
    ret_cols = n_heads * HEAD_DIM
    gated = (
        jax.nn.silu(gate_pre.astype(jnp.float32)) * norm_gain * normed.reshape(tok_rows, ret_cols)
    ).astype(jnp.bfloat16)
    pool_cols = pool_in.shape[1]
    extended = jnp.concatenate([rim_rows, pool_in], axis=0).astype(jnp.float32)
    prefix = jnp.concatenate(
        [jnp.zeros((1, pool_cols), jnp.float32), jnp.cumsum(extended, axis=0)], axis=0
    )
    col_group = (head_index * pool_cols + jnp.arange(pool_cols)) // POOL_GROUP
    counts_base = (positions + 1).astype(jnp.float32)[:, None]
    upper_sum = prefix[16 : 16 + tok_rows]
    selected = jnp.zeros((tok_rows, pool_cols), jnp.float32)
    for group_idx in range(4):
        window_len = 2 ** (group_idx + 1)
        window_mean = (
            upper_sum - prefix[16 - window_len : 16 - window_len + tok_rows]
        ) / jnp.minimum(counts_base, float(window_len))
        selected = jnp.where((col_group == group_idx)[None, :], window_mean, selected)
    pooled = (selected - pool_in.astype(jnp.float32)).astype(jnp.bfloat16)
    ret_rows, pool_rows = (
        lax.all_to_all(gated, "tp", split_axis=0, concat_axis=1, tiled=True),
        lax.all_to_all(pooled, "tp", split_axis=0, concat_axis=1, tiled=True),
    )
    result = jnp.dot(ret_rows, w_out[:RET_WIDTH], preferred_element_type=jnp.float32) + jnp.dot(
        pool_rows, w_out[RET_WIDTH:], preferred_element_type=jnp.float32
    )
    return result.astype(jnp.bfloat16)


def solution(mesh):
    in_specs = (
        P("sp", None),
        P(None, "tp"),
        P(None, "tp"),
        P(None, "tp"),
        P(None, "tp"),
        P(None, "tp"),
        P("tp"),
        P("tp", "sp"),
        P(),
    )
    out_specs = P(("sp", "tp"), None)
    return jax.shard_map(local, mesh=mesh, in_specs=in_specs, out_specs=out_specs, check_vma=False)
```

profile of v0, /device:TPU:1, one launch (start us, length us, event | category | flops | bytes accessed | tf_op | source)
XLA Modules:
  0.0 151.1 jit_solution(8528423157894096770)
XLA Ops:
  0.0 1.3 copy.38
  1.3 23.3 %fusion.77 = f32[16,128,1]{2,0,1:T(8,128)S(1)} fusion(f32[16,128,1]{2,0,1:T(8,128)S(1)} %copy.38), kind=kOutput, calls=%fused_computation.132 | output fusion | flops 260096 | bytes 16384 | tf_op jit(solution)/shard_map/jit(cumsum)/reduce_window_sum | solution.py:82
  25.2 6.3 %fusion.12 = f32[2048,1,128]{0,2,1:T(8,128)S(1)} fusion(bf16[2048,2048]{1,0:T(8,128)(2,1)} %param.11, bf16[2048,128]{1,0:T(8,128)(2,1)S(1)} %copy-done), kind=kOutput, calls=%fused_computation.16 | convolution fusion | flops 1074266112 | bytes 9961472 | tf_op jit(solution)/shard_map/dot_general | solution.py:112
  31.6 6.3 %fusion.14 = f32[2048,1,128]{0,2,1:T(8,128)S(1)} fusion(bf16[2048,2048]{1,0:T(8,128)(2,1)} %param.11, bf16[2048,128]{1,0:T(8,128)(2,1)S(1)} %copy-done.7), kind=kOutput, calls=%fused_computation.18 | convolution fusion | flops 1074266112 | bytes 9961472 | tf_op jit(solution)/shard_map/dot_general | solution.py:112
  37.8 3.0 %fusion.51 = (bf16[2048,1,64]{0,2,1:T(8,128)(2,1)}, bf16[2048,1,64]{0,2,1:T(8,128)(2,1)S(1)}, f32[2048,1,64]{0,2,1:T(8,128)S(1)}, f32[2048,1,64]{0,2,1:T(8,128)S(1)}) fusion(f32[2048,1,128]{0,2,1:T(8,128)S(1)} %fusion.12, f32[64]{0:T(128)S(1)} %multiply_power_fusion, f32[2048]{0:T(1024)S(1)} %fusion.67, f32[2048,1,128]{0,2,1:T(8,128)S(1)} %fusion.14), kind=kLoop, calls=%fused_computation.74 | loop fusion | flops 1966080 | bytes 3678464 | tf_op jit(solution)/shard_map/convert.9
  41.5 6.6 %convolution_convert_fusion.3 = bf16[2048,128]{1,0:T(8,128)(2,1)} fusion(bf16[2048,2048]{1,0:T(8,128)(2,1)} %param.11, bf16[2048,128]{1,0:T(8,128)(2,1)} %param.14), kind=kOutput, calls=%fused_computation.12 | convolution fusion | flops 1074003968 | bytes 9437184 | tf_op jit(solution)/shard_map/dot_general | solution.py:112
  49.2 0.8 convolution_bitcast_fusion.2
  49.9 32.1 %while.13 = (s32[]{:T(128)}, f32[1,128,128]{2,1,0:T(8,128)S(1)}, f32[16,1,128,128]{3,2,1,0:T(8,128)}, f32[16,1]{0,1:T(1,128)S(1)}, f32[16,1,128,128]{3,2,1,0:T(8,128)S(1)}, /*index=5*/s32[]{:T(128)}, s32[]{:T(128)}) while((s32[]{:T(128)}, f32[1,128,128]{2,1,0:T(8,128)S(1)}, f32[16,1,128,128]{3,2,1,0:T(8,128)}, ...), condition=%wide.region_2.3_spmd.clone, body=%wide.region_1.2_spmd.clone.sunk | while | flops 65539 | bytes 328300 | solution.py:141
  51.2 0.7 bitcast_add_fusion.2
  53.2 0.7 bitcast_add_fusion.2
  55.2 0.7 bitcast_add_fusion.2
  83.4 1.1 broadcast_in_dim.58
  84.5 8.6 %all-to-all-start = ((f32[16,129,128]{2,1,0:T(8,128)}), f32[16,129,128]{2,1,0:T(8,128)}, u32[]{:S(2)}, u32[]{:S(2)}) async-start(f32[16,129,128]{2,1,0:T(8,128)} %broadcast_in_dim.58), calls=%async_computation | async-start | bytes 2228224 | tf_op jit(solution)/shard_map/all_to_all | solution.py:20
  93.2 5.8 %convolution_convert_fusion = bf16[2048,128]{1,0:T(8,128)(2,1)S(1)} fusion(bf16[2048,2048]{1,0:T(8,128)(2,1)} %param.11, bf16[2048,128]{1,0:T(8,128)(2,1)S(1)} %copy-done.8), kind=kOutput, calls=%fused_computation.9 | convolution fusion | flops 1074003968 | bytes 9437184 | tf_op jit(solution)/shard_map/dot_general | solution.py:112
  99.0 3.4 %collective-permute-start = (bf16[15,128]{1,0:T(8,128)(2,1)S(1)}, bf16[15,128]{1,0:T(8,128)(2,1)S(1)}, u32[]{:S(2)}, u32[]{:S(2)}) collective-permute-start(bf16[15,128]{1,0:T(8,128)(2,1)S(1)} %slice.158), channel_id=1, source_target_pairs={{0,8},{8,16},{16,24},{24,32},{32,40},{40,48},{48,56},{56,64},{64,7... | collective-permute-start | bytes 11528 | tf_op jit(solution)/shard_map/ppermute | solution.py:15
  102.9 1.0 copy.49
  103.9 0.8 collective-permute-done
  105.0 0.7 fusion.15
  106.2 0.7 copy-done.3
  106.9 1.8 %fusion.41 = bf16[2048,128]{1,0:T(8,128)(2,1)S(1)} fusion(bf16[2048,128]{1,0:T(8,128)(2,1)S(1)} %copy-done.3, f32[2176,128]{1,0:T(8,128)S(1)} %bitcast.113, f32[2063,128]{1,0:T(8,128)S(1)} %slice.162, f32[2048]{0:T(1024)S(1)} %get-tuple-element.98, f32[2048]{0:T(1024)S(1)} %get-tuple-element.99, f32[2048]{0:T(1024)S(1)} %get-tuple-element.100, ...), kind=kLoop, calls=%fused_computation.60 | loop fusion | flops 3932160 | bytes 6332416 | tf_op jit(solution)/shard_map/convert_element_type | solution.py:175
  108.7 1.0 copy.46
  110.0 7.0 %all-to-all-start.2 = ((bf16[8,256,128]{1,2,0:T(8,128)(2,1)}), bf16[8,256,128]{1,2,0:T(8,128)(2,1)}, u32[]{:S(2)}, u32[]{:S(2)}) async-start(bf16[8,256,128]{1,2,0:T(8,128)(2,1)} %copy.46), calls=%async_computation.2 | async-start | bytes 1048576 | tf_op jit(solution)/shard_map/all_to_all | solution.py:178
  116.9 0.8 slice.154
  118.7 1.5 fusion.30
  121.1 1.6 %fusion.18 = f32[16,1,128,128]{2,3,0,1:T(8,128)} fusion(f32[16,1,128,128]{3,2,1,0:T(8,128)S(1)} %copy-done.5, f32[16,128]{1,0:T(8,128)S(1)} %get-tuple-element.88, f32[128,128]{1,0:T(8,128)S(1)} %fusion.65, f32[16]{0:T(128)S(1)} %subtract_exponential_fusion.1, bf16[16,128,64]{2,1,0:T(8,128)(2,1)S(1)} %bitcast.117, bf16[16,128,64]{2,1,0:T(8,128)(2,1)S(1)} %bitcast.115), kind=kOutput, calls=%fused_computation.26 | convolution fusion | flops 69206016 | bytes 2695232 | tf_op jit(solution)/shard_map/nthd,nhde->nthe/dot_general | solution.py:150
  122.7 2.3 %bitcast_reduce_fusion = (f32[16,128]{1,0:T(8,128)S(1)}, f32[16,1,128,128]{2,3,0,1:T(8,128)S(1)}) fusion(f32[16,1,128,128]{2,3,0,1:T(8,128)} %fusion.18, bf16[16,128,128]{2,1,0:T(8,128)(2,1)} %bitcast.123, bf16[16,128,128]{2,1,0:T(8,128)(2,1)S(1)} %fusion.31, f32[16,128]{1,0:T(8,128)S(1)} %bitcast.127, pred[128,128]{1,0:T(8,128)(4,1)S(1)} %iota_compare_fusion, ...), kind=kOutput, calls=%fused_computation.50 | convolution fusion | flops 137099264 | bytes 3702784 | tf_op jit(solution)/shard_map/nhts,nshe->nthe/dot_general | solution.py:91
  125.7 5.9 %fusion.34 = bf16[2048,128]{1,0:T(8,128)(2,1)S(1)} fusion(f32[16,1,128,128]{2,3,0,1:T(8,128)S(1)} %get-tuple-element.97, bf16[2048,2048]{1,0:T(8,128)(2,1)} %param.11, bf16[2048,128]{1,0:T(8,128)(2,1)} %param.15, f32[2048]{0:T(1024)S(1)} %rsqrt_bitcast_fusion, f32[2048]{0:T(1024)S(1)} %get-tuple-element.86, f32[128]{0:T(128)S(1)} %copy-done.9), kind=kOutput, calls=%fused_computation.49 | convolution fusion | flops 1076625408 | bytes 10502656 | tf_op jit(solution)/shard_map/dot_general | solution.py:112
  131.5 1.0 copy.43
  132.5 4.8 %all-to-all-start.1 = ((bf16[8,256,128]{1,2,0:T(8,128)(2,1)}), bf16[8,256,128]{1,2,0:T(8,128)(2,1)S(1)}, u32[]{:S(2)}, u32[]{:S(2)}) async-start(bf16[8,256,128]{1,2,0:T(8,128)(2,1)} %copy.43), calls=%async_computation.1 | async-start | bytes 1048576 | tf_op jit(solution)/shard_map/all_to_all | solution.py:177
  137.3 3.6 %fusion = f32[256,2048]{1,0:T(8,128)S(1)} fusion(bf16[256,1024]{0,1:T(8,128)(2,1)} %bitcast.39, bf16[2048,2048]{1,0:T(8,128)(2,1)} %param.19), kind=kOutput, calls=%fused_computation.3 | convolution fusion | flops 1073741824 | bytes 6815744 | tf_op jit(solution)/shard_map/dot_general | solution.py:180
  141.0 5.7 %all-to-all-done.1 = bf16[8,256,128]{1,2,0:T(8,128)(2,1)S(1)} async-done(((bf16[8,256,128]{1,2,0:T(8,128)(2,1)}), bf16[8,256,128]{1,2,0:T(8,128)(2,1)S(1)}, u32[]{:S(2)}, u32[]{:S(2)}) %all-to-all-start.1) | async-done | bytes 524320 | tf_op jit(solution)/shard_map/all_to_all | solution.py:177
  146.7 4.4 %fusion.7 = bf16[256,2048]{1,0:T(8,128)(2,1)} fusion(f32[256,2048]{1,0:T(8,128)S(1)} %fusion, bf16[256,1024]{0,1:T(8,128)(2,1)S(1)} %bitcast.125, bf16[2048,2048]{1,0:T(8,128)(2,1)} %param.19), kind=kOutput, calls=%fused_computation.8 | convolution fusion | flops 1074790400 | bytes 7864320 | tf_op jit(solution)/shard_map/dot_general | solution.py:180
  (116 shorter events, 36.4 us)
Async XLA Ops:
  0.0 25.2 %copy-start = (bf16[2048,128]{1,0:T(8,128)(2,1)S(1)}, bf16[2048,128]{1,0:T(8,128)(2,1)}, u32[]{:S(2)}) copy-start(bf16[2048,128]{1,0:T(8,128)(2,1)} %param.12) | copy-start | bytes 1572868
  25.2 6.4 %copy-start.7 = (bf16[2048,128]{1,0:T(8,128)(2,1)S(1)}, bf16[2048,128]{1,0:T(8,128)(2,1)}, u32[]{:S(2)}) copy-start(bf16[2048,128]{1,0:T(8,128)(2,1)} %param.13) | copy-start | bytes 1572868
  48.1 1.0 copy-start.4
  82.0 11.1 %copy-start.8 = (bf16[2048,128]{1,0:T(8,128)(2,1)S(1)}, bf16[2048,128]{1,0:T(8,128)(2,1)}, u32[]{:S(2)}) copy-start(bf16[2048,128]{1,0:T(8,128)(2,1)} %param.16) | copy-start | bytes 1572868
  84.5 25.4 %all-to-all-start = ((f32[16,129,128]{2,1,0:T(8,128)}), f32[16,129,128]{2,1,0:T(8,128)}, u32[]{:S(2)}, u32[]{:S(2)}) async-start(f32[16,129,128]{2,1,0:T(8,128)} %broadcast_in_dim.58), calls=%async_computation | async-start | bytes 2228224 | tf_op jit(solution)/shard_map/all_to_all | solution.py:20
  93.2 9.4 %copy-start.6 = (bf16[2048,1,64]{0,2,1:T(8,128)(2,1)S(1)}, bf16[2048,1,64]{0,2,1:T(8,128)(2,1)}, u32[]{:S(2)}) copy-start(bf16[2048,1,64]{0,2,1:T(8,128)(2,1)} %get-tuple-element.78) | copy-start | bytes 786436
  98.9 5.9 %copy-start.2 = (bf16[2048,128]{1,0:T(8,128)(2,1)}, bf16[2048,128]{1,0:T(8,128)(2,1)S(1)}, u32[]{:S(2)}) copy-start(bf16[2048,128]{1,0:T(8,128)(2,1)S(1)} %convolution_convert_fusion) | copy-start | bytes 1572868
  99.0 5.7 %collective-permute-start = (bf16[15,128]{1,0:T(8,128)(2,1)S(1)}, bf16[15,128]{1,0:T(8,128)(2,1)S(1)}, u32[]{:S(2)}, u32[]{:S(2)}) collective-permute-start(bf16[15,128]{1,0:T(8,128)(2,1)S(1)} %slice.158), channel_id=1, source_target_pairs={{0,8},{8,16},{16,24},{24,32},{32,40},{40,48},{48,56},{56,64},{64,7... | collective-permute-start | bytes 11528 | tf_op jit(solution)/shard_map/ppermute | solution.py:15
  105.9 1.0 copy-start.3
  110.0 22.6 %all-to-all-start.2 = ((bf16[8,256,128]{1,2,0:T(8,128)(2,1)}), bf16[8,256,128]{1,2,0:T(8,128)(2,1)}, u32[]{:S(2)}, u32[]{:S(2)}) async-start(bf16[8,256,128]{1,2,0:T(8,128)(2,1)} %copy.46), calls=%async_computation.2 | async-start | bytes 1048576 | tf_op jit(solution)/shard_map/all_to_all | solution.py:178
  118.7 2.4 %copy-start.1 = (bf16[2048,1,64]{2,0,1:T(8,128)(2,1)S(1)}, bf16[2048,1,64]{2,0,1:T(8,128)(2,1)}, u32[]{:S(2)}) copy-start(bf16[2048,1,64]{2,0,1:T(8,128)(2,1)} %copy.49) | copy-start | bytes 786436
  118.7 2.4 %copy-start.5 = (f32[16,1,128,128]{3,2,1,0:T(8,128)S(1)}, f32[16,1,128,128]{3,2,1,0:T(8,128)}, u32[]{:S(2)}) copy-start(f32[16,1,128,128]{3,2,1,0:T(8,128)} %get-tuple-element.33) | copy-start | bytes 3145732
  122.7 3.0 %copy-start.9 = (f32[128]{0:T(128)S(1)}, f32[128]{0:T(128)}, u32[]{:S(2)}) copy-start(f32[128]{0:T(128)} %param.17) | copy-start | bytes 1540
  132.5 14.2 %all-to-all-start.1 = ((bf16[8,256,128]{1,2,0:T(8,128)(2,1)}), bf16[8,256,128]{1,2,0:T(8,128)(2,1)S(1)}, u32[]{:S(2)}, u32[]{:S(2)}) async-start(bf16[8,256,128]{1,2,0:T(8,128)(2,1)} %copy.43), calls=%async_computation.1 | async-start | bytes 1048576 | tf_op jit(solution)/shard_map/all_to_all | solution.py:177
where the time goes:
time: 152 us; the launch traced here: 151 us
  other arithmetic  54.5 us (36%)
  matrix products  43.5 us (29%)
  starting transfers between devices  23.8 us (16%)
  local copies, waits for them, and re-layouts  21.1 us (14%)
  waiting for transfers between devices  6.72 us (4%)
    dot_general x5, matrix products, project(): jnp.dot(tokens, weights, preferred_element_type=jnp.float32)  30.8 us
    another operation x1, other arithmetic, block_parts(): log_cum = jnp.cumsum(decay_blocks, axis=1)  23.3 us
    add x16, other arithmetic, advance(): return (running * jnp.exp(block_end)[:, None, None] + update_n, running)  11 us
    exp x16, local copies, waits for them, and re-layouts, advance(): return (running * jnp.exp(block_end)[:, None, None] + update_n, running)  10.5 us
    dynamic_update_slice x16, other arithmetic, local(): lax.scan(advance, zero_state, (block_ends, updates))  10.3 us
    all_to_all x1, starting transfers between devices, from_everyone(): lax.all_to_all(jnp.broadcast_to(array[None], (peers, *array.shape)), axis...  8.63 us
    all_to_all x1, starting transfers between devices, local(): lax.all_to_all(pooled, 'tp', split_axis=0, concat_axis=1, tiled=True)  6.96 us
    all_to_all x1, waiting for transfers between devices, local(): lax.all_to_all(gated, 'tp', split_axis=0, concat_axis=1, tiled=True)  5.73 us
  transfers between devices with their start and end apart: 4, of which 3 were waited for; matrix products, arithmetic and copies ran while one was open for 20% of the time, Pallas kernels for 0%

commit v1 on v0

v1 whole, which is shorter than its diff:
```python
import functools

import jax
import jax.numpy as jnp
import numpy as np
from jax import lax
from jax.experimental import pallas as pl
from jax.experimental.pallas import tpu as pltpu
from jax.sharding import PartitionSpec as P

HEAD = 128
CHUNK = 256
HALO = 16
F32 = jnp.float32
BF16 = jnp.bfloat16
VMEM_LIMIT = 63 * 1024 * 1024


def dot(a, b):
    return jnp.dot(a, b, preferred_element_type=F32)


def dot_nt(a, b):
    return lax.dot_general(a, b, (((1,), (1,)), ((), ())), preferred_element_type=F32)


def dot_tn(a, b):
    return lax.dot_general(a, b, (((0,), (0,)), ((), ())), preferred_element_type=F32)


def angle_tables(positions):
    half = HEAD // 2
    inverse = 10000.0 ** (-np.arange(half, dtype=np.float64) / half)
    angles = np.asarray(positions, np.float64)[:, None] * inverse[None, :]
    cosine, sine = np.cos(angles), np.sin(angles)
    return (
        np.concatenate([cosine, cosine], axis=1).astype(np.float32),
        np.concatenate([-sine, sine], axis=1).astype(np.float32),
    )


def lane_cumsum(x):
    lane = lax.broadcasted_iota(jnp.int32, x.shape, 1)
    step = 1
    while step < x.shape[1]:
        x = x + jnp.where(lane >= step, pltpu.roll(x, step, 1), 0.0)
        step *= 2
    return x


def kernel(
    n_sp,
    n_tp,
    tok_hbm,
    wq_hbm,
    wk_hbm,
    wv_hbm,
    wg_hbm,
    wp_hbm,
    gain_hbm,
    ld_hbm,
    wout_hbm,
    fine_hbm,
    base_hbm,
    out_hbm,
    x_ref,
    wkv_ref,
    wqg_ref,
    wp_ref,
    wout_ref,
    gain_ref,
    ld_ref,
    fine_ref,
    base_ref,
    k_ref,
    v_ref,
    q_ref,
    g_ref,
    p_ref,
    halo_ref,
    halo_send,
    acc_ref,
    kcol_ref,
    ecol_ref,
    crow_ref,
    ccol_ref,
    be_ref,
    pre_ref,
    state_ref,
    sloc_ref,
    ssend_ref,
    srecv_ref,
    tsend_ref,
    trecv_ref,
    inc_ref,
    psend_ref,
    gsend_ref,
    prow_ref,
    grow_ref,
    oacc_ref,
    obuf_ref,
    tok_sem,
    in_sem,
    wout_sem,
    out_sem,
    tsend_sem,
    trecv_sem,
    ssend_sem,
    srecv_sem,
    hsend_sem,
    hrecv_sem,
    psend_sem,
    precv_sem,
    gsend_sem,
    grecv_sem,
):
    sp = lax.axis_index("sp")
    tp = lax.axis_index("tp")
    rows = x_ref.shape[0]
    n_ch = rows // CHUNK
    width = wout_ref.shape[0] // 2
    n_x = n_tp // 2

    barrier = pltpu.get_barrier_semaphore()
    for j in range(1, n_sp):
        pl.semaphore_signal(barrier, inc=1, device_id={"sp": lax.rem(sp + j, n_sp)})
    for j in range(1, n_tp):
        pl.semaphore_signal(barrier, inc=1, device_id={"tp": lax.rem(tp + j, n_tp)})

    small = [
        pltpu.make_async_copy(ld_hbm, ld_ref, in_sem.at[0]),
        pltpu.make_async_copy(fine_hbm, fine_ref, in_sem.at[1]),
        pltpu.make_async_copy(
            base_hbm.at[:, pl.ds(pl.multiple_of(sp * n_ch, n_ch), n_ch), :], base_ref, in_sem.at[2]
        ),
        pltpu.make_async_copy(gain_hbm, gain_ref, in_sem.at[3]),
    ]
    w_copies = [
        pltpu.make_async_copy(wk_hbm, wkv_ref.at[:, 0:HEAD], in_sem.at[4]),
        pltpu.make_async_copy(wv_hbm, wkv_ref.at[:, HEAD : 2 * HEAD], in_sem.at[5]),
        pltpu.make_async_copy(wp_hbm, wp_ref, in_sem.at[6]),
        pltpu.make_async_copy(wq_hbm, wqg_ref.at[:, 0:HEAD], in_sem.at[7]),
        pltpu.make_async_copy(wg_hbm, wqg_ref.at[:, HEAD : 2 * HEAD], in_sem.at[8]),
    ]

    def chunk_of(c):
        return pl.ds(pl.multiple_of(c * CHUNK, CHUNK), CHUNK)

    def tok_copy(c):
        return pltpu.make_async_copy(
            tok_hbm.at[chunk_of(c), :], x_ref.at[chunk_of(c), :], tok_sem.at[c]
        )

    wout_copy = pltpu.make_async_copy(wout_hbm, wout_ref, wout_sem)

    for copy in small:
        copy.start()
    w_copies[0].start()
    w_copies[1].start()
    for c in range(n_ch):
        tok_copy(c).start()
    for copy in w_copies[2:]:
        copy.start()
    wout_copy.start()

    small[0].wait()
    lc = lane_cumsum(ld_ref[...])
    lct = jnp.transpose(lc)
    run = jnp.zeros((1, 1), F32)
    for c in range(n_ch):
        a, b = 2 * c, 2 * c + 1
        end_a = lc[a : a + 1, HEAD - 1 :]
        end = end_a + lc[b : b + 1, HEAD - 1 :]
        crow_ref[c, 0:1, :] = jnp.concatenate([lc[a : a + 1, :], lc[b : b + 1, :] + end_a], axis=1)
        col = jnp.concatenate(
            [
                jnp.broadcast_to(lct[:, a : a + 1], (HEAD, HEAD)),
                jnp.broadcast_to(lct[:, b : b + 1] + end_a, (HEAD, HEAD)),
            ],
            axis=0,
        )
        here = slice(c * CHUNK, (c + 1) * CHUNK)
        ccol_ref[here, :] = col
        kcol_ref[here, :] = jnp.exp(end - col)
        ecol_ref[here, :] = jnp.exp(col)
        be_ref[c : c + 1, :] = jnp.broadcast_to(jnp.exp(end), (1, HEAD))
        pre_ref[c : c + 1, :] = jnp.broadcast_to(jnp.exp(run), (1, HEAD))
        run = run + end
    tsend_ref[...] = jnp.broadcast_to(run, tsend_ref.shape)

    pl.semaphore_wait(barrier, n_sp - 1 + n_tp - 1)

    def t_copy(j):
        return pltpu.make_async_remote_copy(
            src_ref=tsend_ref,
            dst_ref=trecv_ref.at[sp],
            send_sem=tsend_sem.at[j],
            recv_sem=trecv_sem.at[sp],
            device_id={"sp": lax.rem(sp + j, n_sp)},
            device_id_type=pl.DeviceIdType.MESH,
        )

    def s_copy(j):
        return pltpu.make_async_remote_copy(
            src_ref=ssend_ref,
            dst_ref=srecv_ref.at[sp],
            send_sem=ssend_sem.at[j],
            recv_sem=srecv_sem.at[sp],
            device_id={"sp": lax.rem(sp + j, n_sp)},
            device_id_type=pl.DeviceIdType.MESH,
        )

    for j in range(1, n_sp):

        @pl.when(sp + j < n_sp)
        def _():
            t_copy(j).start()

    small[1].wait()
    small[2].wait()
    w_copies[0].wait()
    w_copies[1].wait()
    state_ref[...] = jnp.zeros_like(state_ref)

    def turned(x, c):
        base_c = base_ref[0, pl.ds(c, 1), :]
        base_s = base_ref[1, pl.ds(c, 1), :]
        fine_c = fine_ref[0]
        fine_s = fine_ref[1]
        cosine = base_c * fine_c - base_s * fine_s
        sine = base_s * fine_c + base_c * fine_s
        return x * cosine + pltpu.roll(x, HEAD // 2, 1) * sine

    def kv_step(c, carry):
        tok_copy(c).wait()
        here = chunk_of(c)
        kv = dot(x_ref[here, :], wkv_ref[...])
        key = kv[:, :HEAD].astype(BF16).astype(F32)
        value = kv[:, HEAD:].astype(BF16)
        k_rot = (turned(key, c) * HEAD**-0.5).astype(BF16)
        k_ref[here, :] = k_rot
        v_ref[here, :] = value
        decayed = (k_rot.astype(F32) * kcol_ref[here, :]).astype(BF16)
        update = dot_tn(decayed, value)
        state = state_ref[...]
        sloc_ref[c] = state.astype(BF16)
        state_ref[...] = state * be_ref[pl.ds(c, 1), :] + update
        return carry

    lax.fori_loop(0, n_ch, kv_step, 0)
    ssend_ref[...] = state_ref[...].astype(BF16)
    for j in range(1, n_sp):

        @pl.when(sp + j < n_sp)
        def _():
            s_copy(j).start()

    w_copies[2].wait()

    def p_of(c):
        here = chunk_of(c)
        p = dot(x_ref[here, :], wp_ref[...]).astype(BF16)
        p_ref[pl.ds(pl.multiple_of(HALO + c * CHUNK, HALO), CHUNK), :] = p.astype(F32)
        return p

    halo_copy = pltpu.make_async_remote_copy(
        src_ref=halo_send,
        dst_ref=halo_ref,
        send_sem=hsend_sem,
        recv_sem=hrecv_sem,
        device_id={"sp": lax.rem(sp + 1, n_sp)},
        device_id_type=pl.DeviceIdType.MESH,
    )
    halo_send[...] = p_of(n_ch - 1)[CHUNK - HALO :, :]

    @pl.when(sp + 1 < n_sp)
    def _():
        halo_copy.start()

    def p_step(c, carry):
        p_of(c)
        return carry

    lax.fori_loop(0, n_ch - 1, p_step, 0)

    @pl.when(sp > 0)
    def _():
        halo_copy.wait_recv()
        p_ref[0:HALO, :] = halo_ref[...].astype(F32)

    @pl.when(sp == 0)
    def _():
        p_ref[0:HALO, :] = jnp.zeros((HALO, HEAD), F32)

    x_at, core = lax.div(tp, 2), lax.rem(tp, 2)
    order = [(2, 0), (3, 0), (2, 1), (3, 1), (1, 0), (1, 1), (0, 1), (0, 0)]

    def peer_of(dx, dc):
        return lax.rem(x_at + dx, n_x) * 2 + lax.rem(core + dc, 2)

    def row_copy(k, send_ref, recv_ref, send_sem, recv_sem):
        peer = peer_of(*order[k])
        return pltpu.make_async_remote_copy(
            src_ref=send_ref.at[peer],
            dst_ref=recv_ref.at[tp],
            send_sem=send_sem.at[k],
            recv_sem=recv_sem.at[tp],
            device_id={"tp": peer},
            device_id_type=pl.DeviceIdType.MESH,
        )

    def recv_wait(j, send_ref, recv_ref, send_sem, recv_sem):
        pltpu.make_async_remote_copy(
            src_ref=send_ref.at[0],
            dst_ref=recv_ref.at[j],
            send_sem=send_sem.at[0],
            recv_sem=recv_sem.at[j],
            device_id={"tp": tp},
            device_id_type=pl.DeviceIdType.MESH,
        ).wait_recv()

    group = lax.div(tp * HEAD, 256)
    window = jnp.left_shift(jnp.int32(2), group)

    def pooled_of(c):
        x = p_ref[pl.ds(pl.multiple_of(c * CHUNK, CHUNK), CHUNK + HALO), :]
        s = x + pltpu.roll(x, 1, 0)
        for level in (1, 2, 3):
            s = jnp.where(group >= level, s + pltpu.roll(s, 2**level, 0), s)
        s = s[HALO:, :]
        x = x[HALO:, :]
        at = lax.broadcasted_iota(jnp.int32, (HALO, HEAD), 0) + (sp * rows + c * CHUNK + 1)
        count = jnp.minimum(at, window).astype(F32)
        whole = jnp.minimum(lax.broadcasted_iota(jnp.int32, (1, HEAD), 1) + 4096, window).astype(F32)
        top = s[:HALO, :] / count
        rest = s[HALO:, :] * (1.0 / whole)
        return (jnp.concatenate([top, rest], axis=0) - x).astype(BF16)

    p_args = (psend_ref, prow_ref, psend_sem, precv_sem)
    g_args = (gsend_ref, grow_ref, gsend_sem, grecv_sem)
    for k in range(n_tp - 1):
        peer = peer_of(*order[k])
        psend_ref[peer] = pooled_of(peer)
        row_copy(k, *p_args).start()
    prow_ref[tp] = pooled_of(tp)

    w_copies[3].wait()
    w_copies[4].wait()
    tri = lax.broadcasted_iota(jnp.int32, (CHUNK, CHUNK), 0) >= lax.broadcasted_iota(
        jnp.int32, (CHUNK, CHUNK), 1
    )

    def q_step(c, carry):
        here = chunk_of(c)
        qg = dot(x_ref[here, :], wqg_ref[...])
        query = qg[:, :HEAD].astype(BF16).astype(F32)
        g_ref[here, :] = qg[:, HEAD:].astype(BF16)
        q_rot = turned(query, c).astype(BF16)
        q_ref[here, :] = q_rot
        scores = dot_nt(q_rot, k_ref[here, :])
        col = ccol_ref[here, :]
        gap = jnp.concatenate([col, col], axis=1) - crow_ref[c, 0:1, :]
        weights = jnp.where(tri, jnp.exp(jnp.minimum(gap, 0.0)), 0.0)
        mixing = (scores * weights).astype(BF16)
        inner = dot(mixing, v_ref[here, :])
        cross = dot(q_rot, sloc_ref[c]) * ecol_ref[here, :]
        acc_ref[here, :] = inner + cross
        return carry

    lax.fori_loop(0, n_ch, q_step, 0)

    inc_ref[...] = jnp.zeros_like(inc_ref)

    def inc_step(j, carry):
        t_wait = pltpu.make_async_remote_copy(
            src_ref=tsend_ref,
            dst_ref=trecv_ref.at[j],
            send_sem=tsend_sem.at[0],
            recv_sem=trecv_sem.at[j],
            device_id={"sp": sp},
            device_id_type=pl.DeviceIdType.MESH,
        )
        s_wait = pltpu.make_async_remote_copy(
            src_ref=ssend_ref,
            dst_ref=srecv_ref.at[j],
            send_sem=ssend_sem.at[0],
            recv_sem=srecv_sem.at[j],
            device_id={"sp": sp},
            device_id_type=pl.DeviceIdType.MESH,
        )
        t_wait.wait_recv()
        s_wait.wait_recv()
        inc_ref[...] = inc_ref[...] * jnp.exp(trecv_ref[j, 0:1, :]) + srecv_ref[j].astype(F32)
        return carry

    lax.fori_loop(0, sp, inc_step, 0)
    incoming = inc_ref[...].astype(BF16)

    small[3].wait()

    def gated_of(c):
        here = chunk_of(c)
        cross = dot(q_ref[here, :], incoming) * (ecol_ref[here, :] * pre_ref[pl.ds(c, 1), :])
        retained = acc_ref[here, :] + cross
        centered = retained - jnp.mean(retained, axis=-1, keepdims=True)
        scale = lax.rsqrt(jnp.mean(centered * centered, axis=-1, keepdims=True) + 1e-06)
        gate = g_ref[here, :].astype(F32)
        return (gate * jax.nn.sigmoid(gate) * gain_ref[...] * (centered * scale)).astype(BF16)

    for k in range(n_tp - 1):
        peer = peer_of(*order[k])
        gsend_ref[peer] = gated_of(peer)
        row_copy(k, *g_args).start()
    grow_ref[tp] = gated_of(tp)

    wout_copy.wait()
    for j in range(n_tp):

        @pl.when(tp != j)
        def _():
            recv_wait(j, *p_args)

    n_cols = wout_ref.shape[1]
    tile = 256
    pool_rows = jnp.concatenate([prow_ref[j] for j in range(n_tp)], axis=1)

    def pool_step(i, carry):
        at = pl.ds(pl.multiple_of(i * tile, tile), tile)
        oacc_ref[:, at] = dot(pool_rows, wout_ref[pl.ds(width, width), at])
        return carry

    lax.fori_loop(0, n_cols // tile, pool_step, 0)

    def out_copy(i):
        at = pl.ds(pl.multiple_of(i * tile, tile), tile)
        return pltpu.make_async_copy(obuf_ref.at[:, at], out_hbm.at[:, at], out_sem.at[i])

    for n, dx in enumerate((0, 1, 3, 2)):
        pair = lax.rem(x_at + dx, n_x)
        if dx == 0:
            recv_wait(pair * 2 + 1 - core, *g_args)
        else:
            recv_wait(pair * 2, *g_args)
            recv_wait(pair * 2 + 1, *g_args)
        lhs = jnp.concatenate([grow_ref[pair * 2], grow_ref[pair * 2 + 1]], axis=1)
        deep = pl.ds(pl.multiple_of(pair * 2 * HEAD, 2 * HEAD), 2 * HEAD)

        def out_step(i, carry):
            at = pl.ds(pl.multiple_of(i * tile, tile), tile)
            total = oacc_ref[:, at] + dot(lhs, wout_ref[deep, at])
            if n < 3:
                oacc_ref[:, at] = total
            else:
                obuf_ref[:, at] = total.astype(BF16)
                out_copy(i).start()
            return carry

        lax.fori_loop(0, n_cols // tile, out_step, 0)

    for j in range(1, n_sp):

        @pl.when(sp + j < n_sp)
        def _():
            t_copy(j).wait_send()
            s_copy(j).wait_send()

    @pl.when(sp + 1 < n_sp)
    def _():
        halo_copy.wait_send()

    for k in range(n_tp - 1):
        row_copy(k, *p_args).wait_send()
        row_copy(k, *g_args).wait_send()
    for i in range(n_cols // tile):
        out_copy(i).wait()


def local(n_sp, n_tp, tokens, w_query, w_key, w_value, w_gate, w_pool, norm_gain, log_decay, w_out):
    rows, depth = tokens.shape
    n_ch = rows // CHUNK
    out_rows, out_cols = rows // n_tp, w_out.shape[1]
    fine = np.stack(angle_tables(np.arange(CHUNK)))
    base = np.stack(angle_tables(np.arange(n_sp * n_ch) * CHUNK))
    any_spec = pl.BlockSpec(memory_space=pl.ANY)
    dma = pltpu.SemaphoreType.DMA
    vm = pltpu.VMEM
    return pl.pallas_call(
        functools.partial(kernel, n_sp, n_tp),
        out_shape=jax.ShapeDtypeStruct((out_rows, out_cols), BF16),
        in_specs=[any_spec] * 11,
        out_specs=any_spec,
        scratch_shapes=[
            vm((rows, depth), BF16),
            vm((depth, 2 * HEAD), BF16),
            vm((depth, 2 * HEAD), BF16),
            vm((depth, HEAD), BF16),
            vm(w_out.shape, BF16),
            vm((1, HEAD), F32),
            vm((rows // HEAD, HEAD), F32),
            vm((2, CHUNK, HEAD), F32),
            vm((2, n_ch, HEAD), F32),
            vm((rows, HEAD), BF16),
            vm((rows, HEAD), BF16),
            vm((rows, HEAD), BF16),
            vm((rows, HEAD), BF16),
            vm((rows + HALO, HEAD), F32),
            vm((HALO, HEAD), BF16),
            vm((HALO, HEAD), BF16),
            vm((rows, HEAD), F32),
            vm((rows, HEAD), F32),
            vm((rows, HEAD), F32),
            vm((n_ch, 8, CHUNK), F32),
            vm((rows, HEAD), F32),
            vm((n_ch, HEAD), F32),
            vm((n_ch, HEAD), F32),
            vm((HEAD, HEAD), F32),
            vm((n_ch, HEAD, HEAD), BF16),
            vm((HEAD, HEAD), BF16),
            vm((n_sp, HEAD, HEAD), BF16),
            vm((8, HEAD), F32),
            vm((n_sp, 8, HEAD), F32),
            vm((HEAD, HEAD), F32),
            vm((n_tp, CHUNK, HEAD), BF16),
            vm((n_tp, CHUNK, HEAD), BF16),
            vm((n_tp, CHUNK, HEAD), BF16),
            vm((n_tp, CHUNK, HEAD), BF16),
            vm((out_rows, out_cols), F32),
            vm((out_rows, out_cols), BF16),
            dma((n_ch,)),
            dma((9,)),
            dma,
            dma((out_cols // 256,)),
            dma((n_sp,)),
            dma((n_sp,)),
            dma((n_sp,)),
            dma((n_sp,)),
            dma,
            dma,
            dma((n_tp,)),
            dma((n_tp,)),
            dma((n_tp,)),
            dma((n_tp,)),
        ],
        compiler_params=pltpu.CompilerParams(
            collective_id=0, has_side_effects=True, vmem_limit_bytes=VMEM_LIMIT
        ),
        name="layer",
    )(
        tokens,
        w_query,
        w_key,
        w_value,
        w_gate,
        w_pool,
        norm_gain.reshape(1, HEAD),
        log_decay.reshape(rows // HEAD, HEAD),
        w_out,
        fine,
        base,
    )


def solution(mesh):
    in_specs = (
        P("sp", None),
        P(None, "tp"),
        P(None, "tp"),
        P(None, "tp"),
        P(None, "tp"),
        P(None, "tp"),
        P("tp"),
        P("tp", "sp"),
        P(),
    )
    body = functools.partial(local, mesh.shape["sp"], mesh.shape["tp"])
    return jax.shard_map(
        body, mesh=mesh, in_specs=in_specs, out_specs=P(("sp", "tp"), None), check_vma=False
    )
```

time: 152 us -> 42.9 us (0.28)
  the two profiles are of different devices: /device:TPU:1 before, /device:TPU:11 now
where the time goes in v1:
time: 42.9 us; the launch traced here: 42.8 us
  Pallas kernels  40.5 us (94%)
  local copies, waits for them, and re-layouts  2.3 us (5%)
    pallas_call x1, Pallas kernels, local(): pl.pallas_call(functools.partial(kernel, n_sp, n_tp), out_shape=jax.Shape...  40.5 us
    unnamed x1, local copies, waits for them, and re-layouts  2.3 us

profile of v1, /device:TPU:11, one launch (start us, length us, event | category | flops | bytes accessed | tf_op | source)
XLA Modules:
  0.0 42.8 jit_solution(12802864734646060187)
XLA Ops:
  0.0 40.5 %layer.1 = bf16[256,2048]{1,0:T(8,128)(2,1)} custom-call(bf16[2048,2048]{1,0:T(8,128)(2,1)} %tok_hbm.1, bf16[2048,128]{1,0:T(8,128)(2,1)} %wq_hbm.1, bf16[2048,128]{1,0:T(8,128)(2,1)} %wk_hbm.1, bf16[2048,128]{1,0:T(8,128)(2,1)} %wv_hbm.1, bf16[2048,128]{1,0:T(8,128)(2,1)} %wg_hbm.1, bf16[2048,128]{1,0:T(8,128)(2,1)} %wp_hbm.1, f32[1,128]{1,0:T(1,128)} %bitcast.3, ...), custom_call_target="tpu_custom_call" | custom-call | tf_op jit(solution)/shard_map/layer/pallas_call | solution.py:487
  40.5 2.3 %copy.13 = bf16[256,2048]{1,0:T(8,128)(2,1)} copy(bf16[256,2048]{1,0:T(8,128)(2,1)} %layer.1) | data formatting | bytes 2097152

commit v2 on v1

--- a/solution.py
+++ b/solution.py
@@ -13,7 +13,7 @@
 HALO = 16
 F32 = jnp.float32
 BF16 = jnp.bfloat16
-VMEM_LIMIT = 63 * 1024 * 1024
+VMEM_LIMIT = 62 * 1024 * 1024 + 512 * 1024
 
 
 def dot(a, b):
@@ -62,7 +62,7 @@
     wout_hbm,
     fine_hbm,
     base_hbm,
-    out_hbm,
+    obuf_ref,
     x_ref,
     wkv_ref,
     wqg_ref,
@@ -86,7 +86,6 @@
     ccol_ref,
     be_ref,
     pre_ref,
-    state_ref,
     sloc_ref,
     ssend_ref,
     srecv_ref,
@@ -98,11 +97,9 @@
     prow_ref,
     grow_ref,
     oacc_ref,
-    obuf_ref,
     tok_sem,
     in_sem,
     wout_sem,
-    out_sem,
     tsend_sem,
     trecv_sem,
     ssend_sem,
@@ -144,6 +141,8 @@
     ]
 
     def chunk_of(c):
+        if isinstance(c, int):
+            return slice(c * CHUNK, (c + 1) * CHUNK)
         return pl.ds(pl.multiple_of(c * CHUNK, CHUNK), CHUNK)
 
     def tok_copy(c):
@@ -153,15 +152,13 @@
 
     wout_copy = pltpu.make_async_copy(wout_hbm, wout_ref, wout_sem)
 
-    for copy in small:
-        copy.start()
+    small[0].start()
     w_copies[0].start()
     w_copies[1].start()
+    small[1].start()
+    small[2].start()
     for c in range(n_ch):
         tok_copy(c).start()
-    for copy in w_copies[2:]:
-        copy.start()
-    wout_copy.start()
 
     small[0].wait()
     lc = lane_cumsum(ld_ref[...])
@@ -188,8 +185,6 @@
         run = run + end
     tsend_ref[...] = jnp.broadcast_to(run, tsend_ref.shape)
 
-    pl.semaphore_wait(barrier, n_sp - 1 + n_tp - 1)
-
     def t_copy(j):
         return pltpu.make_async_remote_copy(
             src_ref=tsend_ref,
@@ -210,17 +205,10 @@
             device_id_type=pl.DeviceIdType.MESH,
         )
 
-    for j in range(1, n_sp):
-
-        @pl.when(sp + j < n_sp)
-        def _():
-            t_copy(j).start()
-
     small[1].wait()
     small[2].wait()
     w_copies[0].wait()
     w_copies[1].wait()
-    state_ref[...] = jnp.zeros_like(state_ref)
 
     def turned(x, c):
         base_c = base_ref[0, pl.ds(c, 1), :]
@@ -231,10 +219,18 @@
         sine = base_s * fine_c + base_c * fine_s
         return x * cosine + pltpu.roll(x, HEAD // 2, 1) * sine
 
-    def kv_step(c, carry):
-        tok_copy(c).wait()
+    def kv_of(c):
+        if c % 2 == 0:
+            tok_copy(c).wait()
+            tok_copy(c + 1).wait()
+        if c == 4:
+            for copy in w_copies[2:]:
+                copy.start()
+            small[3].start()
+        return dot(x_ref[chunk_of(c), :], wkv_ref[...])
+
+    def keep_kv(c, kv, state):
         here = chunk_of(c)
-        kv = dot(x_ref[here, :], wkv_ref[...])
         key = kv[:, :HEAD].astype(BF16).astype(F32)
         value = kv[:, HEAD:].astype(BF16)
         k_rot = (turned(key, c) * HEAD**-0.5).astype(BF16)
@@ -242,17 +238,25 @@
         v_ref[here, :] = value
         decayed = (k_rot.astype(F32) * kcol_ref[here, :]).astype(BF16)
         update = dot_tn(decayed, value)
-        state = state_ref[...]
         sloc_ref[c] = state.astype(BF16)
-        state_ref[...] = state * be_ref[pl.ds(c, 1), :] + update
-        return carry
-
-    lax.fori_loop(0, n_ch, kv_step, 0)
-    ssend_ref[...] = state_ref[...].astype(BF16)
+        return state * be_ref[pl.ds(c, 1), :] + update
+
+    state = jnp.zeros((HEAD, HEAD), F32)
+    kv = kv_of(0)
+    for c in range(n_ch):
+        if c + 1 < n_ch:
+            kv_next = kv_of(c + 1)
+        state = keep_kv(c, kv, state)
+        kv = kv_next
+    wout_copy.start()
+    ssend_ref[...] = state.astype(BF16)
+
+    pl.semaphore_wait(barrier, n_sp - 1 + n_tp - 1)
     for j in range(1, n_sp):
 
         @pl.when(sp + j < n_sp)
         def _():
+            t_copy(j).start()
             s_copy(j).start()
 
     w_copies[2].wait()
@@ -260,7 +264,7 @@
     def p_of(c):
         here = chunk_of(c)
         p = dot(x_ref[here, :], wp_ref[...]).astype(BF16)
-        p_ref[pl.ds(pl.multiple_of(HALO + c * CHUNK, HALO), CHUNK), :] = p.astype(F32)
+        p_ref[HALO + c * CHUNK : HALO + (c + 1) * CHUNK, :] = p.astype(F32)
         return p
 
     halo_copy = pltpu.make_async_remote_copy(
@@ -271,26 +275,15 @@
         device_id={"sp": lax.rem(sp + 1, n_sp)},
         device_id_type=pl.DeviceIdType.MESH,
     )
+    p_ref[0:HALO, :] = jnp.zeros((HALO, HEAD), F32)
     halo_send[...] = p_of(n_ch - 1)[CHUNK - HALO :, :]
 
     @pl.when(sp + 1 < n_sp)
     def _():
         halo_copy.start()
 
-    def p_step(c, carry):
+    for c in range(n_ch - 1):
         p_of(c)
-        return carry
-
-    lax.fori_loop(0, n_ch - 1, p_step, 0)
-
-    @pl.when(sp > 0)
-    def _():
-        halo_copy.wait_recv()
-        p_ref[0:HALO, :] = halo_ref[...].astype(F32)
-
-    @pl.when(sp == 0)
-    def _():
-        p_ref[0:HALO, :] = jnp.zeros((HALO, HEAD), F32)
 
     x_at, core = lax.div(tp, 2), lax.rem(tp, 2)
     order = [(2, 0), (3, 0), (2, 1), (3, 1), (1, 0), (1, 1), (0, 1), (0, 0)]
@@ -298,12 +291,11 @@
     def peer_of(dx, dc):
         return lax.rem(x_at + dx, n_x) * 2 + lax.rem(core + dc, 2)
 
-    def row_copy(k, send_ref, recv_ref, send_sem, recv_sem):
-        peer = peer_of(*order[k])
+    def row_copy(peer, send_ref, recv_ref, send_sem, recv_sem):
         return pltpu.make_async_remote_copy(
             src_ref=send_ref.at[peer],
             dst_ref=recv_ref.at[tp],
-            send_sem=send_sem.at[k],
+            send_sem=send_sem.at[peer],
             recv_sem=recv_sem.at[tp],
             device_id={"tp": peer},
             device_id_type=pl.DeviceIdType.MESH,
@@ -341,7 +333,11 @@
     for k in range(n_tp - 1):
         peer = peer_of(*order[k])
         psend_ref[peer] = pooled_of(peer)
-        row_copy(k, *p_args).start()
+
+        @pl.when(peer != 0)
+        def _():
+            row_copy(peer, *p_args).start()
+
     prow_ref[tp] = pooled_of(tp)
 
     w_copies[3].wait()
@@ -350,9 +346,8 @@
         jnp.int32, (CHUNK, CHUNK), 1
     )
 
-    def q_step(c, carry):
+    def keep_q(c, qg):
         here = chunk_of(c)
-        qg = dot(x_ref[here, :], wqg_ref[...])
         query = qg[:, :HEAD].astype(BF16).astype(F32)
         g_ref[here, :] = qg[:, HEAD:].astype(BF16)
         q_rot = turned(query, c).astype(BF16)
@@ -365,9 +360,28 @@
         inner = dot(mixing, v_ref[here, :])
         cross = dot(q_rot, sloc_ref[c]) * ecol_ref[here, :]
         acc_ref[here, :] = inner + cross
-        return carry
-
-    lax.fori_loop(0, n_ch, q_step, 0)
+
+    qg = dot(x_ref[chunk_of(0), :], wqg_ref[...])
+    for c in range(n_ch):
+        if c + 1 < n_ch:
+            qg_next = dot(x_ref[chunk_of(c + 1), :], wqg_ref[...])
+        keep_q(c, qg)
+        qg = qg_next
+
+    @pl.when(sp > 0)
+    def _():
+        halo_copy.wait_recv()
+        p_ref[0:HALO, :] = halo_ref[...].astype(F32)
+    first = pooled_of(0)
+
+    @pl.when(tp == 0)
+    def _():
+        prow_ref[0] = first
+
+    @pl.when(tp != 0)
+    def _():
+        psend_ref[0] = first
+        row_copy(0, *p_args).start()
 
     inc_ref[...] = jnp.zeros_like(inc_ref)
 
@@ -410,7 +424,7 @@
     for k in range(n_tp - 1):
         peer = peer_of(*order[k])
         gsend_ref[peer] = gated_of(peer)
-        row_copy(k, *g_args).start()
+        row_copy(peer, *g_args).start()
     grow_ref[tp] = gated_of(tp)
 
     wout_copy.wait()
@@ -431,11 +445,7 @@
 
     lax.fori_loop(0, n_cols // tile, pool_step, 0)
 
-    def out_copy(i):
-        at = pl.ds(pl.multiple_of(i * tile, tile), tile)
-        return pltpu.make_async_copy(obuf_ref.at[:, at], out_hbm.at[:, at], out_sem.at[i])
-
-    for n, dx in enumerate((0, 1, 3, 2)):
+    for n, dx in enumerate((0, 2, 1, 3)):
         pair = lax.rem(x_at + dx, n_x)
         if dx == 0:
             recv_wait(pair * 2 + 1 - core, *g_args)
@@ -452,7 +462,6 @@
                 oacc_ref[:, at] = total
             else:
                 obuf_ref[:, at] = total.astype(BF16)
-                out_copy(i).start()
             return carry
 
         lax.fori_loop(0, n_cols // tile, out_step, 0)
@@ -469,10 +478,9 @@
         halo_copy.wait_send()
 
     for k in range(n_tp - 1):
-        row_copy(k, *p_args).wait_send()
-        row_copy(k, *g_args).wait_send()
-    for i in range(n_cols // tile):
-        out_copy(i).wait()
+        peer = peer_of(*order[k])
+        row_copy(peer, *p_args).wait_send()
+        row_copy(peer, *g_args).wait_send()
 
 
 def local(n_sp, n_tp, tokens, w_query, w_key, w_value, w_gate, w_pool, norm_gain, log_decay, w_out):
@@ -481,14 +489,14 @@
     out_rows, out_cols = rows // n_tp, w_out.shape[1]
     fine = np.stack(angle_tables(np.arange(CHUNK)))
     base = np.stack(angle_tables(np.arange(n_sp * n_ch) * CHUNK))
-    any_spec = pl.BlockSpec(memory_space=pl.ANY)
+    any_spec = pl.BlockSpec(memory_space=pltpu.HBM)
     dma = pltpu.SemaphoreType.DMA
     vm = pltpu.VMEM
     return pl.pallas_call(
         functools.partial(kernel, n_sp, n_tp),
-        out_shape=jax.ShapeDtypeStruct((out_rows, out_cols), BF16),
+        out_shape=pltpu.VMEM((out_rows, out_cols), BF16),
         in_specs=[any_spec] * 11,
-        out_specs=any_spec,
+        out_specs=pl.BlockSpec(memory_space=pltpu.VMEM),
         scratch_shapes=[
             vm((rows, depth), BF16),
             vm((depth, 2 * HEAD), BF16),
@@ -513,7 +521,6 @@
             vm((rows, HEAD), F32),
             vm((n_ch, HEAD), F32),
             vm((n_ch, HEAD), F32),
-            vm((HEAD, HEAD), F32),
             vm((n_ch, HEAD, HEAD), BF16),
             vm((HEAD, HEAD), BF16),
             vm((n_sp, HEAD, HEAD), BF16),
@@ -525,11 +532,9 @@
             vm((n_tp, CHUNK, HEAD), BF16),
             vm((n_tp, CHUNK, HEAD), BF16),
             vm((out_rows, out_cols), F32),
-            vm((out_rows, out_cols), BF16),
             dma((n_ch,)),
             dma((9,)),
             dma,
-            dma((out_cols // 256,)),
             dma((n_sp,)),
             dma((n_sp,)),
             dma((n_sp,)),
@@ -558,8 +563,6 @@
         fine,
         base,
     )
-
-
 def solution(mesh):
     in_specs = (
         P("sp", None),

time: 42.9 us -> 35 us (0.82)
  the two profiles are of different devices: /device:TPU:11 before, /device:TPU:0 now
where the time goes in v2:
time: 35 us; the launch traced here: 34.9 us
  Pallas kernels  33.9 us (97%)
  local copies, waits for them, and re-layouts  0.97 us (3%)
    pallas_call x1, Pallas kernels, local(): pl.pallas_call(functools.partial(kernel, n_sp, n_tp), out_shape=pltpu.VME...  33.9 us
    unnamed x1, local copies, waits for them, and re-layouts  0.97 us

profile of v2, /device:TPU:0, one launch (start us, length us, event | category | flops | bytes accessed | tf_op | source)
XLA Modules:
  0.0 34.9 jit_solution(1828213736121203757)
XLA Ops:
  0.0 33.9 %layer.1 = bf16[256,2048]{1,0:T(8,128)(2,1)S(1)} custom-call(bf16[2048,2048]{1,0:T(8,128)(2,1)} %tok_hbm.1, bf16[2048,128]{1,0:T(8,128)(2,1)} %wq_hbm.1, bf16[2048,128]{1,0:T(8,128)(2,1)} %wk_hbm.1, bf16[2048,128]{1,0:T(8,128)(2,1)} %wv_hbm.1, bf16[2048,128]{1,0:T(8,128)(2,1)} %wg_hbm.1, bf16[2048,128]{1,0:T(8,128)(2,1)} %wp_hbm.1, f32[1,128]{1,0:T(1,128)} %bitcast.3, ...), custom_call_target="tpu_custom_call" | custom-call | tf_op jit(solution)/shard_map/layer/pallas_call | solution.py:495
  33.9 1.0 %copy.13 = bf16[256,2048]{1,0:T(8,128)(2,1)} copy(bf16[256,2048]{1,0:T(8,128)(2,1)S(1)} %layer.1) | data formatting | bytes 2097152

commit v3 on v2

--- a/solution.py
+++ b/solution.py
@@ -11,6 +11,8 @@
 HEAD = 128
 CHUNK = 256
 HALO = 16
+SIDE = 4
+ROW_AT = 0
 F32 = jnp.float32
 BF16 = jnp.bfloat16
 VMEM_LIMIT = 62 * 1024 * 1024 + 512 * 1024
@@ -80,10 +82,10 @@
     halo_ref,
     halo_send,
     acc_ref,
-    kcol_ref,
+    lc_ref,
+    lct_ref,
     ecol_ref,
-    crow_ref,
-    ccol_ref,
+    d_ref,
     be_ref,
     pre_ref,
     sloc_ref,
@@ -91,6 +93,12 @@
     srecv_ref,
     tsend_ref,
     trecv_ref,
+    rsend_ref,
+    rrecv_ref,
+    usend_ref,
+    urecv_ref,
+    pref_ref,
+    upto_ref,
     inc_ref,
     psend_ref,
     gsend_ref,
@@ -104,6 +112,10 @@
     trecv_sem,
     ssend_sem,
     srecv_sem,
+    rsend_sem,
+    rrecv_sem,
+    usend_sem,
+    urecv_sem,
     hsend_sem,
     hrecv_sem,
     psend_sem,
@@ -119,8 +131,21 @@
     n_x = n_tp // 2
 
     barrier = pltpu.get_barrier_semaphore()
-    for j in range(1, n_sp):
-        pl.semaphore_signal(barrier, inc=1, device_id={"sp": lax.rem(sp + j, n_sp)})
+    n_y = SIDE
+    n_z = n_sp // n_y
+    z, y = lax.div(sp, n_y), lax.rem(sp, n_y)
+
+    def row_peer(j):
+        return z * n_y + lax.rem(y + j, n_y)
+
+    def column_peer(j):
+        return lax.rem(z + j, n_z) * n_y + y
+
+    sp_peers = [row_peer(j) for j in range(1, n_y)]
+    sp_peers += [column_peer(j) for j in range(1, n_z)]
+    sp_peers += [lax.rem(sp + 1, n_sp), lax.rem(sp + n_sp - 1, n_sp)]
+    for peer in sp_peers:
+        pl.semaphore_signal(barrier, inc=1, device_id={"sp": peer})
     for j in range(1, n_tp):
         pl.semaphore_signal(barrier, inc=1, device_id={"tp": lax.rem(tp + j, n_tp)})
 
@@ -152,57 +177,66 @@
 
     wout_copy = pltpu.make_async_copy(wout_hbm, wout_ref, wout_sem)
 
-    small[0].start()
+    for copy in small[:3]:
+        copy.start()
     w_copies[0].start()
     w_copies[1].start()
-    small[1].start()
-    small[2].start()
-    for c in range(n_ch):
-        tok_copy(c).start()
+    tok_copy(0).start()
+    tok_copy(1).start()
 
     small[0].wait()
+    tok_copy(2).start()
+    tok_copy(3).start()
     lc = lane_cumsum(ld_ref[...])
-    lct = jnp.transpose(lc)
+    lc_ref[...] = lc
+    lct_ref[...] = jnp.transpose(lc)
     run = jnp.zeros((1, 1), F32)
     for c in range(n_ch):
-        a, b = 2 * c, 2 * c + 1
-        end_a = lc[a : a + 1, HEAD - 1 :]
-        end = end_a + lc[b : b + 1, HEAD - 1 :]
-        crow_ref[c, 0:1, :] = jnp.concatenate([lc[a : a + 1, :], lc[b : b + 1, :] + end_a], axis=1)
-        col = jnp.concatenate(
-            [
-                jnp.broadcast_to(lct[:, a : a + 1], (HEAD, HEAD)),
-                jnp.broadcast_to(lct[:, b : b + 1] + end_a, (HEAD, HEAD)),
-            ],
-            axis=0,
-        )
-        here = slice(c * CHUNK, (c + 1) * CHUNK)
-        ccol_ref[here, :] = col
-        kcol_ref[here, :] = jnp.exp(end - col)
-        ecol_ref[here, :] = jnp.exp(col)
+        end = lc[2 * c : 2 * c + 1, HEAD - 1 :] + lc[2 * c + 1 : 2 * c + 2, HEAD - 1 :]
         be_ref[c : c + 1, :] = jnp.broadcast_to(jnp.exp(end), (1, HEAD))
         pre_ref[c : c + 1, :] = jnp.broadcast_to(jnp.exp(run), (1, HEAD))
         run = run + end
     tsend_ref[...] = jnp.broadcast_to(run, tsend_ref.shape)
 
-    def t_copy(j):
+    def columns(c):
+        first = jnp.broadcast_to(lct_ref[:, 2 * c : 2 * c + 1], (HEAD, HEAD))
+        second = jnp.broadcast_to(lct_ref[:, 2 * c + 1 : 2 * c + 2], (HEAD, HEAD))
+        return first, second + lc_ref[2 * c : 2 * c + 1, HEAD - 1 :]
+
+    def decay_of_chunk(c):
+        row_a = lc_ref[2 * c : 2 * c + 1, :]
+        row_b = lc_ref[2 * c + 1 : 2 * c + 2, :] + row_a[:, HEAD - 1 :]
+        col_a, col_b = columns(c)
+        low = lax.broadcasted_iota(jnp.int32, (HEAD, HEAD), 0) >= lax.broadcasted_iota(
+            jnp.int32, (HEAD, HEAD), 1
+        )
+        d_ref[c, :HEAD, :HEAD] = jnp.where(low, jnp.exp(jnp.minimum(col_a - row_a, 0.0)), 0.0)
+        d_ref[c, :HEAD, HEAD:] = jnp.zeros((HEAD, HEAD), F32)
+        d_ref[c, HEAD:, :HEAD] = jnp.exp(col_b - row_a)
+        d_ref[c, HEAD:, HEAD:] = jnp.where(low, jnp.exp(jnp.minimum(col_b - row_b, 0.0)), 0.0)
+        ecol_ref[c * CHUNK : c * CHUNK + HEAD, :] = jnp.exp(col_a)
+        ecol_ref[c * CHUNK + HEAD : (c + 1) * CHUNK, :] = jnp.exp(col_b)
+
+    def pushed(src, dst, slot, peer, send_sem, recv_sem, at):
         return pltpu.make_async_remote_copy(
-            src_ref=tsend_ref,
-            dst_ref=trecv_ref.at[sp],
-            send_sem=tsend_sem.at[j],
-            recv_sem=trecv_sem.at[sp],
-            device_id={"sp": lax.rem(sp + j, n_sp)},
+            src_ref=src,
+            dst_ref=dst.at[slot],
+            send_sem=send_sem.at[at],
+            recv_sem=recv_sem.at[slot],
+            device_id={"sp": peer},
             device_id_type=pl.DeviceIdType.MESH,
         )
 
-    def s_copy(j):
-        return pltpu.make_async_remote_copy(
-            src_ref=ssend_ref,
-            dst_ref=srecv_ref.at[sp],
-            send_sem=ssend_sem.at[j],
-            recv_sem=srecv_sem.at[sp],
-            device_id={"sp": lax.rem(sp + j, n_sp)},
-            device_id_type=pl.DeviceIdType.MESH,
+    def row_sends(j):
+        return (
+            pushed(tsend_ref, trecv_ref, y, row_peer(j), tsend_sem, trecv_sem, j),
+            pushed(ssend_ref, srecv_ref, y, row_peer(j), ssend_sem, srecv_sem, j),
+        )
+
+    def column_sends(j):
+        return (
+            pushed(usend_ref, urecv_ref, z, column_peer(j), usend_sem, urecv_sem, j),
+            pushed(rsend_ref, rrecv_ref, z, column_peer(j), rsend_sem, rrecv_sem, j),
         )
 
     small[1].wait()
@@ -220,11 +254,19 @@
         return x * cosine + pltpu.roll(x, HEAD // 2, 1) * sine
 
     def kv_of(c):
-        if c % 2 == 0:
-            tok_copy(c).wait()
-            tok_copy(c + 1).wait()
+        if c == 0:
+            tok_copy(0).wait()
+            tok_copy(1).wait()
+            for later in range(4, n_ch):
+                tok_copy(later).start()
+            w_copies[2].start()
+        if c == 2:
+            tok_copy(2).wait()
+            tok_copy(3).wait()
         if c == 4:
-            for copy in w_copies[2:]:
+            for later in range(4, n_ch):
+                tok_copy(later).wait()
+            for copy in w_copies[3:]:
                 copy.start()
             small[3].start()
         return dot(x_ref[chunk_of(c), :], wkv_ref[...])
@@ -236,7 +278,10 @@
         k_rot = (turned(key, c) * HEAD**-0.5).astype(BF16)
         k_ref[here, :] = k_rot
         v_ref[here, :] = value
-        decayed = (k_rot.astype(F32) * kcol_ref[here, :]).astype(BF16)
+        col_a, col_b = columns(c)
+        end = col_b[HEAD - 1 :, :]
+        fade = jnp.concatenate([jnp.exp(end - col_a), jnp.exp(end - col_b)], axis=0)
+        decayed = (k_rot.astype(F32) * fade).astype(BF16)
         update = dot_tn(decayed, value)
         sloc_ref[c] = state.astype(BF16)
         return state * be_ref[pl.ds(c, 1), :] + update
@@ -249,24 +294,13 @@
         state = keep_kv(c, kv, state)
         kv = kv_next
     wout_copy.start()
+    w_copies[2].wait()
+    halo_send[...] = dot(x_ref[rows - HALO :, :], wp_ref[...]).astype(BF16)
     ssend_ref[...] = state.astype(BF16)
-
-    pl.semaphore_wait(barrier, n_sp - 1 + n_tp - 1)
-    for j in range(1, n_sp):
-
-        @pl.when(sp + j < n_sp)
-        def _():
-            t_copy(j).start()
-            s_copy(j).start()
-
-    w_copies[2].wait()
-
-    def p_of(c):
-        here = chunk_of(c)
-        p = dot(x_ref[here, :], wp_ref[...]).astype(BF16)
-        p_ref[HALO + c * CHUNK : HALO + (c + 1) * CHUNK, :] = p.astype(F32)
-        return p
-
+    srecv_ref[y] = state.astype(BF16)
+    trecv_ref[y] = tsend_ref[...]
+
+    pl.semaphore_wait(barrier, len(sp_peers) + n_tp - 1)
     halo_copy = pltpu.make_async_remote_copy(
         src_ref=halo_send,
         dst_ref=halo_ref,
@@ -275,15 +309,14 @@
         device_id={"sp": lax.rem(sp + 1, n_sp)},
         device_id_type=pl.DeviceIdType.MESH,
     )
-    p_ref[0:HALO, :] = jnp.zeros((HALO, HEAD), F32)
-    halo_send[...] = p_of(n_ch - 1)[CHUNK - HALO :, :]
 
     @pl.when(sp + 1 < n_sp)
     def _():
         halo_copy.start()
 
-    for c in range(n_ch - 1):
-        p_of(c)
+    for j in (2, 1, 3):
+        for copy in row_sends(j):
+            copy.start()
 
     x_at, core = lax.div(tp, 2), lax.rem(tp, 2)
     order = [(2, 0), (3, 0), (2, 1), (3, 1), (1, 0), (1, 1), (0, 1), (0, 0)]
@@ -315,7 +348,7 @@
     window = jnp.left_shift(jnp.int32(2), group)
 
     def pooled_of(c):
-        x = p_ref[pl.ds(pl.multiple_of(c * CHUNK, CHUNK), CHUNK + HALO), :]
+        x = p_ref[c * CHUNK : (c + 1) * CHUNK + HALO, :]
         s = x + pltpu.roll(x, 1, 0)
         for level in (1, 2, 3):
             s = jnp.where(group >= level, s + pltpu.roll(s, 2**level, 0), s)
@@ -330,22 +363,36 @@
 
     p_args = (psend_ref, prow_ref, psend_sem, precv_sem)
     g_args = (gsend_ref, grow_ref, gsend_sem, grecv_sem)
+
+    def p_of(c):
+        return dot(x_ref[chunk_of(c), :], wp_ref[...])
+
+    p = p_of(0)
+    for c in range(n_ch):
+        if c + 1 < n_ch:
+            p_next = p_of(c + 1)
+        p_ref[HALO + c * CHUNK : HALO + (c + 1) * CHUNK, :] = p.astype(BF16).astype(F32)
+        decay_of_chunk(c)
+        if c > 0:
+            psend_ref[c] = pooled_of(c)
+        p = p_next
+
+    @pl.when(sp > 0)
+    def _():
+        halo_copy.wait_recv()
+        p_ref[0:HALO, :] = halo_ref[...].astype(F32)
+
+    @pl.when(sp == 0)
+    def _():
+        p_ref[0:HALO, :] = jnp.zeros((HALO, HEAD), F32)
+
+    psend_ref[0] = pooled_of(0)
     for k in range(n_tp - 1):
-        peer = peer_of(*order[k])
-        psend_ref[peer] = pooled_of(peer)
-
-        @pl.when(peer != 0)
-        def _():
-            row_copy(peer, *p_args).start()
-
-    prow_ref[tp] = pooled_of(tp)
+        row_copy(peer_of(*order[k]), *p_args).start()
+    prow_ref[tp] = psend_ref[tp]
 
     w_copies[3].wait()
     w_copies[4].wait()
-    tri = lax.broadcasted_iota(jnp.int32, (CHUNK, CHUNK), 0) >= lax.broadcasted_iota(
-        jnp.int32, (CHUNK, CHUNK), 1
-    )
-
     def keep_q(c, qg):
         here = chunk_of(c)
         query = qg[:, :HEAD].astype(BF16).astype(F32)
@@ -353,13 +400,36 @@
         q_rot = turned(query, c).astype(BF16)
         q_ref[here, :] = q_rot
         scores = dot_nt(q_rot, k_ref[here, :])
-        col = ccol_ref[here, :]
-        gap = jnp.concatenate([col, col], axis=1) - crow_ref[c, 0:1, :]
-        weights = jnp.where(tri, jnp.exp(jnp.minimum(gap, 0.0)), 0.0)
-        mixing = (scores * weights).astype(BF16)
+        mixing = (scores * d_ref[c]).astype(BF16)
         inner = dot(mixing, v_ref[here, :])
         cross = dot(q_rot, sloc_ref[c]) * ecol_ref[here, :]
         acc_ref[here, :] = inner + cross
+
+    def row_states():
+        for j in range(1, n_y):
+            slot = lax.rem(y + j, n_y)
+            pushed(tsend_ref, trecv_ref, slot, sp, tsend_sem, trecv_sem, 0).wait_recv()
+            pushed(ssend_ref, srecv_ref, slot, sp, ssend_sem, srecv_sem, 0).wait_recv()
+        total = jnp.zeros((HEAD, HEAD), F32)
+        before = jnp.zeros((HEAD, HEAD), F32)
+        reach = jnp.zeros((1, HEAD), F32)
+        upto = jnp.zeros((1, HEAD), F32)
+        for j in range(n_y):
+            before = jnp.where(y == j, total, before)
+            upto = jnp.where(y == j, reach, upto)
+            decay = trecv_ref[j, 0:1, :]
+            total = total * jnp.exp(decay) + srecv_ref[j].astype(F32)
+            reach = reach + decay
+        pref_ref[...] = before
+        upto_ref[...] = jnp.broadcast_to(jnp.exp(upto), upto_ref.shape)
+        usend_ref[...] = jnp.broadcast_to(reach, usend_ref.shape)
+        rsend_ref[...] = total.astype(BF16)
+        for j in range(1, n_z):
+
+            @pl.when(z + j < n_z)
+            def _():
+                for copy in column_sends(j):
+                    copy.start()
 
     qg = dot(x_ref[chunk_of(0), :], wqg_ref[...])
     for c in range(n_ch):
@@ -367,48 +437,19 @@
             qg_next = dot(x_ref[chunk_of(c + 1), :], wqg_ref[...])
         keep_q(c, qg)
         qg = qg_next
-
-    @pl.when(sp > 0)
-    def _():
-        halo_copy.wait_recv()
-        p_ref[0:HALO, :] = halo_ref[...].astype(F32)
-    first = pooled_of(0)
-
-    @pl.when(tp == 0)
-    def _():
-        prow_ref[0] = first
-
-    @pl.when(tp != 0)
-    def _():
-        psend_ref[0] = first
-        row_copy(0, *p_args).start()
+        if c == ROW_AT:
+            row_states()
 
     inc_ref[...] = jnp.zeros_like(inc_ref)
 
     def inc_step(j, carry):
-        t_wait = pltpu.make_async_remote_copy(
-            src_ref=tsend_ref,
-            dst_ref=trecv_ref.at[j],
-            send_sem=tsend_sem.at[0],
-            recv_sem=trecv_sem.at[j],
-            device_id={"sp": sp},
-            device_id_type=pl.DeviceIdType.MESH,
-        )
-        s_wait = pltpu.make_async_remote_copy(
-            src_ref=ssend_ref,
-            dst_ref=srecv_ref.at[j],
-            send_sem=ssend_sem.at[0],
-            recv_sem=srecv_sem.at[j],
-            device_id={"sp": sp},
-            device_id_type=pl.DeviceIdType.MESH,
-        )
-        t_wait.wait_recv()
-        s_wait.wait_recv()
-        inc_ref[...] = inc_ref[...] * jnp.exp(trecv_ref[j, 0:1, :]) + srecv_ref[j].astype(F32)
+        pushed(usend_ref, urecv_ref, j, sp, usend_sem, urecv_sem, 0).wait_recv()
+        pushed(rsend_ref, rrecv_ref, j, sp, rsend_sem, rrecv_sem, 0).wait_recv()
+        inc_ref[...] = inc_ref[...] * jnp.exp(urecv_ref[j, 0:1, :]) + rrecv_ref[j].astype(F32)
         return carry
 
-    lax.fori_loop(0, sp, inc_step, 0)
-    incoming = inc_ref[...].astype(BF16)
+    lax.fori_loop(0, z, inc_step, 0)
+    incoming = (inc_ref[...] * upto_ref[0:1, :] + pref_ref[...]).astype(BF16)
 
     small[3].wait()
 
@@ -438,12 +479,9 @@
     tile = 256
     pool_rows = jnp.concatenate([prow_ref[j] for j in range(n_tp)], axis=1)
 
-    def pool_step(i, carry):
-        at = pl.ds(pl.multiple_of(i * tile, tile), tile)
-        oacc_ref[:, at] = dot(pool_rows, wout_ref[pl.ds(width, width), at])
-        return carry
-
-    lax.fori_loop(0, n_cols // tile, pool_step, 0)
+    tiles = [slice(i * tile, (i + 1) * tile) for i in range(n_cols // tile)]
+    for at in tiles:
+        oacc_ref[:, at] = dot(pool_rows, wout_ref[width:, at])
 
     for n, dx in enumerate((0, 2, 1, 3)):
         pair = lax.rem(x_at + dx, n_x)
@@ -455,23 +493,22 @@
         lhs = jnp.concatenate([grow_ref[pair * 2], grow_ref[pair * 2 + 1]], axis=1)
         deep = pl.ds(pl.multiple_of(pair * 2 * HEAD, 2 * HEAD), 2 * HEAD)
 
-        def out_step(i, carry):
-            at = pl.ds(pl.multiple_of(i * tile, tile), tile)
+        for at in tiles:
             total = oacc_ref[:, at] + dot(lhs, wout_ref[deep, at])
             if n < 3:
                 oacc_ref[:, at] = total
             else:
                 obuf_ref[:, at] = total.astype(BF16)
-            return carry
-
-        lax.fori_loop(0, n_cols // tile, out_step, 0)
-
-    for j in range(1, n_sp):
-
-        @pl.when(sp + j < n_sp)
+
+    for j in range(1, n_y):
+        for copy in row_sends(j):
+            copy.wait_send()
+    for j in range(1, n_z):
+
+        @pl.when(z + j < n_z)
         def _():
-            t_copy(j).wait_send()
-            s_copy(j).wait_send()
+            for copy in column_sends(j):
+                copy.wait_send()
 
     @pl.when(sp + 1 < n_sp)
     def _():
@@ -515,17 +552,23 @@
             vm((HALO, HEAD), BF16),
             vm((HALO, HEAD), BF16),
             vm((rows, HEAD), F32),
+            vm((rows // HEAD, HEAD), F32),
+            vm((HEAD, rows // HEAD), F32),
             vm((rows, HEAD), F32),
-            vm((rows, HEAD), F32),
-            vm((n_ch, 8, CHUNK), F32),
-            vm((rows, HEAD), F32),
+            vm((n_ch, CHUNK, CHUNK), F32),
             vm((n_ch, HEAD), F32),
             vm((n_ch, HEAD), F32),
             vm((n_ch, HEAD, HEAD), BF16),
             vm((HEAD, HEAD), BF16),
-            vm((n_sp, HEAD, HEAD), BF16),
+            vm((SIDE, HEAD, HEAD), BF16),
             vm((8, HEAD), F32),
-            vm((n_sp, 8, HEAD), F32),
+            vm((SIDE, 8, HEAD), F32),
+            vm((HEAD, HEAD), BF16),
+            vm((n_sp // SIDE, HEAD, HEAD), BF16),
+            vm((8, HEAD), F32),
+            vm((n_sp // SIDE, 8, HEAD), F32),
+            vm((HEAD, HEAD), F32),
+            vm((8, HEAD), F32),
             vm((HEAD, HEAD), F32),
             vm((n_tp, CHUNK, HEAD), BF16),
             vm((n_tp, CHUNK, HEAD), BF16),
@@ -535,10 +578,14 @@
             dma((n_ch,)),
             dma((9,)),
             dma,
-            dma((n_sp,)),
-            dma((n_sp,)),
-            dma((n_sp,)),
-            dma((n_sp,)),
+            dma((SIDE,)),
+            dma((SIDE,)),
+            dma((SIDE,)),
+            dma((SIDE,)),
+            dma((n_sp // SIDE,)),
+            dma((n_sp // SIDE,)),
+            dma((n_sp // SIDE,)),
+            dma((n_sp // SIDE,)),
             dma,
             dma,
             dma((n_tp,)),

time: 35 us -> 27.9 us (0.80)
  the two profiles are of different devices: /device:TPU:0 before, /device:TPU:1 now
where the time goes in v3:
time: 27.9 us; the launch traced here: 27.8 us
  Pallas kernels  26.8 us (96%)
  local copies, waits for them, and re-layouts  0.97 us (3%)
    pallas_call x1, Pallas kernels, local(): pl.pallas_call(functools.partial(kernel, n_sp, n_tp), out_shape=pltpu.VME...  26.8 us
    unnamed x1, local copies, waits for them, and re-layouts  0.97 us

profile of v3, /device:TPU:1, one launch (start us, length us, event | category | flops | bytes accessed | tf_op | source)
XLA Modules:
  0.0 27.8 jit_solution(15513883977591682535)
XLA Ops:
  0.0 26.8 %layer.1 = bf16[256,2048]{1,0:T(8,128)(2,1)S(1)} custom-call(bf16[2048,2048]{1,0:T(8,128)(2,1)} %tok_hbm.1, bf16[2048,128]{1,0:T(8,128)(2,1)} %wq_hbm.1, bf16[2048,128]{1,0:T(8,128)(2,1)} %wk_hbm.1, bf16[2048,128]{1,0:T(8,128)(2,1)} %wv_hbm.1, bf16[2048,128]{1,0:T(8,128)(2,1)} %wg_hbm.1, bf16[2048,128]{1,0:T(8,128)(2,1)} %wp_hbm.1, f32[1,128]{1,0:T(1,128)} %bitcast.3, ...), custom_call_target="tpu_custom_call" | custom-call | tf_op jit(solution)/shard_map/layer/pallas_call | solution.py:532
  26.8 1.0 %copy.13 = bf16[256,2048]{1,0:T(8,128)(2,1)} copy(bf16[256,2048]{1,0:T(8,128)(2,1)S(1)} %layer.1) | data formatting | bytes 2097152

commit v4 on v3

--- a/solution.py
+++ b/solution.py
@@ -12,7 +12,11 @@
 CHUNK = 256
 HALO = 16
 SIDE = 4
-ROW_AT = 0
+PAD = 8
+EARLY = 4
+LOG_SCALE = -0.5 * float(np.log(HEAD))
+ROW_AT = 3
+HALO_AT = 2
 F32 = jnp.float32
 BF16 = jnp.bfloat16
 VMEM_LIMIT = 62 * 1024 * 1024 + 512 * 1024
@@ -76,6 +80,7 @@
     base_ref,
     k_ref,
     v_ref,
+    faded_ref,
     q_ref,
     g_ref,
     p_ref,
@@ -84,7 +89,12 @@
     acc_ref,
     lc_ref,
     lct_ref,
+    cos_ref,
+    sin_ref,
+    fade_ref,
+    shift_ref,
     ecol_ref,
+    edev_ref,
     d_ref,
     be_ref,
     pre_ref,
@@ -125,7 +135,7 @@
 ):
     sp = lax.axis_index("sp")
     tp = lax.axis_index("tp")
-    rows = x_ref.shape[0]
+    rows = x_ref.shape[0] - HALO
     n_ch = rows // CHUNK
     width = wout_ref.shape[0] // 2
     n_x = n_tp // 2
@@ -143,9 +153,18 @@
 
     sp_peers = [row_peer(j) for j in range(1, n_y)]
     sp_peers += [column_peer(j) for j in range(1, n_z)]
-    sp_peers += [lax.rem(sp + 1, n_sp), lax.rem(sp + n_sp - 1, n_sp)]
     for peer in sp_peers:
         pl.semaphore_signal(barrier, inc=1, device_id={"sp": peer})
+
+    @pl.when(sp + 1 < n_sp)
+    def _():
+        pl.semaphore_signal(barrier, inc=1, device_id={"sp": lax.rem(sp + 1, n_sp)})
+
+    @pl.when(sp > 0)
+    def _():
+        pl.semaphore_signal(barrier, inc=1, device_id={"sp": lax.rem(sp + n_sp - 1, n_sp)})
+
+    met = len(sp_peers) + n_tp - 1 + jnp.minimum(sp, 1) + jnp.minimum(n_sp - 1 - sp, 1)
     for j in range(1, n_tp):
         pl.semaphore_signal(barrier, inc=1, device_id={"tp": lax.rem(tp + j, n_tp)})
 
@@ -170,9 +189,12 @@
             return slice(c * CHUNK, (c + 1) * CHUNK)
         return pl.ds(pl.multiple_of(c * CHUNK, CHUNK), CHUNK)
 
+    def x_rows(c):
+        return slice(HALO + c * CHUNK, HALO + (c + 1) * CHUNK)
+
     def tok_copy(c):
         return pltpu.make_async_copy(
-            tok_hbm.at[chunk_of(c), :], x_ref.at[chunk_of(c), :], tok_sem.at[c]
+            tok_hbm.at[chunk_of(c), :], x_ref.at[x_rows(c), :], tok_sem.at[c]
         )
 
     wout_copy = pltpu.make_async_copy(wout_hbm, wout_ref, wout_sem)
@@ -185,6 +207,7 @@
     tok_copy(1).start()
 
     small[0].wait()
+    w_copies[2].start()
     tok_copy(2).start()
     tok_copy(3).start()
     lc = lane_cumsum(ld_ref[...])
@@ -210,12 +233,15 @@
         low = lax.broadcasted_iota(jnp.int32, (HEAD, HEAD), 0) >= lax.broadcasted_iota(
             jnp.int32, (HEAD, HEAD), 1
         )
-        d_ref[c, :HEAD, :HEAD] = jnp.where(low, jnp.exp(jnp.minimum(col_a - row_a, 0.0)), 0.0)
+        sc_a, sc_b = col_a + LOG_SCALE, col_b + LOG_SCALE
+        d_ref[c, :HEAD, :HEAD] = jnp.where(low, jnp.exp(sc_a - row_a), 0.0)
         d_ref[c, :HEAD, HEAD:] = jnp.zeros((HEAD, HEAD), F32)
-        d_ref[c, HEAD:, :HEAD] = jnp.exp(col_b - row_a)
-        d_ref[c, HEAD:, HEAD:] = jnp.where(low, jnp.exp(jnp.minimum(col_b - row_b, 0.0)), 0.0)
-        ecol_ref[c * CHUNK : c * CHUNK + HEAD, :] = jnp.exp(col_a)
-        ecol_ref[c * CHUNK + HEAD : (c + 1) * CHUNK, :] = jnp.exp(col_b)
+        d_ref[c, HEAD:, :HEAD] = jnp.exp(sc_b - row_a)
+        d_ref[c, HEAD:, HEAD:] = jnp.where(low, jnp.exp(sc_b - row_b), 0.0)
+        here = chunk_of(c)
+        within = jnp.exp(jnp.concatenate([col_a, col_b], axis=0))
+        ecol_ref[here, :] = within
+        edev_ref[here, :] = within * pre_ref[c : c + 1, :]
 
     def pushed(src, dst, slot, peer, send_sem, recv_sem, at):
         return pltpu.make_async_remote_copy(
@@ -241,25 +267,110 @@
 
     small[1].wait()
     small[2].wait()
+    for c in range(n_ch):
+        here = chunk_of(c)
+        base_c = base_ref[0, c : c + 1, :]
+        base_s = base_ref[1, c : c + 1, :]
+        fine_c = fine_ref[0]
+        fine_s = fine_ref[1]
+        cos_ref[here, :] = base_c * fine_c - base_s * fine_s
+        sin_ref[here, :] = base_s * fine_c + base_c * fine_s
+        col_a, col_b = columns(c)
+        end = col_b[HEAD - 1 :, :] + LOG_SCALE
+        fade_ref[here, :] = jnp.exp(jnp.concatenate([end - col_a, end - col_b], axis=0))
+    p_ref[0 : PAD + HALO, :] = jnp.zeros((PAD + HALO, HEAD), F32)
+    shift_ref[0:PAD, :] = jnp.zeros((PAD, HEAD), F32)
+    for later in range(4, n_ch):
+        tok_copy(later).start()
     w_copies[0].wait()
     w_copies[1].wait()
+    w_copies[2].wait()
 
     def turned(x, c):
-        base_c = base_ref[0, pl.ds(c, 1), :]
-        base_s = base_ref[1, pl.ds(c, 1), :]
-        fine_c = fine_ref[0]
-        fine_s = fine_ref[1]
-        cosine = base_c * fine_c - base_s * fine_s
-        sine = base_s * fine_c + base_c * fine_s
-        return x * cosine + pltpu.roll(x, HEAD // 2, 1) * sine
+        here = chunk_of(c)
+        return x * cos_ref[here, :] + pltpu.roll(x, HEAD // 2, 1) * sin_ref[here, :]
+
+    x_at, core = lax.div(tp, 2), lax.rem(tp, 2)
+    order = [(1, 0), (3, 0), (2, 0), (2, 1), (1, 1), (3, 1), (0, 1), (0, 0)]
+
+    def peer_of(dx, dc):
+        return lax.rem(x_at + dx, n_x) * 2 + lax.rem(core + dc, 2)
+
+    def row_copy(peer, send_ref, recv_ref, send_sem, recv_sem):
+        return pltpu.make_async_remote_copy(
+            src_ref=send_ref.at[peer],
+            dst_ref=recv_ref.at[tp],
+            send_sem=send_sem.at[peer],
+            recv_sem=recv_sem.at[tp],
+            device_id={"tp": peer},
+            device_id_type=pl.DeviceIdType.MESH,
+        )
+
+    def recv_wait(j, send_ref, recv_ref, send_sem, recv_sem):
+        pltpu.make_async_remote_copy(
+            src_ref=send_ref.at[0],
+            dst_ref=recv_ref.at[j],
+            send_sem=send_sem.at[0],
+            recv_sem=recv_sem.at[j],
+            device_id={"tp": tp},
+            device_id_type=pl.DeviceIdType.MESH,
+        ).wait_recv()
+
+    group = lax.div(tp * HEAD, 256)
+    window = jnp.left_shift(jnp.int32(2), group)
+
+    def pooled_of(c):
+        deep = CHUNK + HALO
+        at = PAD + c * CHUNK
+        x = p_ref[at : at + deep, :]
+        s = x + p_ref[at - 1 : at - 1 + deep, :]
+        for level in (1, 2, 3):
+            shift_ref[PAD : PAD + deep, :] = s
+            back = shift_ref[PAD - 2**level : PAD - 2**level + deep, :]
+            s = jnp.where(group >= level, s + back, s)
+        s = s[HALO:, :]
+        x = x[HALO:, :]
+        at = lax.broadcasted_iota(jnp.int32, (HALO, HEAD), 0) + (sp * rows + c * CHUNK + 1)
+        count = jnp.minimum(at, window).astype(F32)
+        whole = jnp.minimum(lax.broadcasted_iota(jnp.int32, (1, HEAD), 1) + 4096, window).astype(F32)
+        top = s[:HALO, :] / count
+        rest = s[HALO:, :] * (1.0 / whole)
+        return (jnp.concatenate([top, rest], axis=0) - x).astype(BF16)
+
+    p_args = (psend_ref, prow_ref, psend_sem, precv_sem)
+    g_args = (gsend_ref, grow_ref, gsend_sem, grecv_sem)
+
+    def p_of(c):
+        return dot(x_ref[x_rows(c), :], wp_ref[...])
+
+    def keep_p(c, p):
+        p_ref[PAD + HALO + c * CHUNK : PAD + HALO + (c + 1) * CHUNK, :] = p
+        if c > 0:
+            psend_ref[c] = pooled_of(c)
+
+    def send_pooled(*chunks):
+        for c in chunks:
+
+            @pl.when(tp != c)
+            def _():
+                row_copy(c, *p_args).start()
+
+    def first_chunk():
+        @pl.when(sp > 0)
+        def _():
+            halo_copy.wait_recv()
+            p_ref[PAD : PAD + HALO, :] = halo_ref[...].astype(F32)
+
+        psend_ref[0] = pooled_of(0)
+        send_pooled(0)
+        prow_ref[tp] = psend_ref[tp]
+
+    peers = [peer_of(dx, dc) for dx, dc in order]
 
     def kv_of(c):
         if c == 0:
             tok_copy(0).wait()
             tok_copy(1).wait()
-            for later in range(4, n_ch):
-                tok_copy(later).start()
-            w_copies[2].start()
         if c == 2:
             tok_copy(2).wait()
             tok_copy(3).wait()
@@ -269,38 +380,41 @@
             for copy in w_copies[3:]:
                 copy.start()
             small[3].start()
-        return dot(x_ref[chunk_of(c), :], wkv_ref[...])
-
-    def keep_kv(c, kv, state):
+            pl.semaphore_wait(barrier, met)
+            send_pooled(*range(1, 3))
+        return dot(x_ref[x_rows(c), :], wkv_ref[...])
+
+    def keep_kv(c, kv):
         here = chunk_of(c)
-        key = kv[:, :HEAD].astype(BF16).astype(F32)
-        value = kv[:, HEAD:].astype(BF16)
-        k_rot = (turned(key, c) * HEAD**-0.5).astype(BF16)
-        k_ref[here, :] = k_rot
-        v_ref[here, :] = value
-        col_a, col_b = columns(c)
-        end = col_b[HEAD - 1 :, :]
-        fade = jnp.concatenate([jnp.exp(end - col_a), jnp.exp(end - col_b)], axis=0)
-        decayed = (k_rot.astype(F32) * fade).astype(BF16)
-        update = dot_tn(decayed, value)
+        k_rot = turned(kv[:, :HEAD], c)
+        k_ref[here, :] = k_rot.astype(BF16)
+        v_ref[here, :] = kv[:, HEAD:].astype(BF16)
+        faded_ref[c] = jnp.transpose((k_rot * fade_ref[here, :]).astype(BF16))
+
+    def advance(c, state):
         sloc_ref[c] = state.astype(BF16)
-        return state * be_ref[pl.ds(c, 1), :] + update
+        return state * be_ref[c : c + 1, :] + dot(faded_ref[c], v_ref[chunk_of(c), :])
 
     state = jnp.zeros((HEAD, HEAD), F32)
     kv = kv_of(0)
     for c in range(n_ch):
         if c + 1 < n_ch:
             kv_next = kv_of(c + 1)
-        state = keep_kv(c, kv, state)
+        if c > 0:
+            state = advance(c - 1, state)
+        if c < EARLY:
+            p = p_of(c)
+        keep_kv(c, kv)
+        if c < EARLY:
+            keep_p(c, p)
         kv = kv_next
+    state = advance(n_ch - 1, state)
     wout_copy.start()
-    w_copies[2].wait()
-    halo_send[...] = dot(x_ref[rows - HALO :, :], wp_ref[...]).astype(BF16)
+    halo_send[...] = dot(x_ref[rows:, :], wp_ref[...]).astype(BF16)
     ssend_ref[...] = state.astype(BF16)
     srecv_ref[y] = state.astype(BF16)
     trecv_ref[y] = tsend_ref[...]
 
-    pl.semaphore_wait(barrier, len(sp_peers) + n_tp - 1)
     halo_copy = pltpu.make_async_remote_copy(
         src_ref=halo_send,
         dst_ref=halo_ref,
@@ -318,92 +432,32 @@
         for copy in row_sends(j):
             copy.start()
 
-    x_at, core = lax.div(tp, 2), lax.rem(tp, 2)
-    order = [(2, 0), (3, 0), (2, 1), (3, 1), (1, 0), (1, 1), (0, 1), (0, 0)]
-
-    def peer_of(dx, dc):
-        return lax.rem(x_at + dx, n_x) * 2 + lax.rem(core + dc, 2)
-
-    def row_copy(peer, send_ref, recv_ref, send_sem, recv_sem):
-        return pltpu.make_async_remote_copy(
-            src_ref=send_ref.at[peer],
-            dst_ref=recv_ref.at[tp],
-            send_sem=send_sem.at[peer],
-            recv_sem=recv_sem.at[tp],
-            device_id={"tp": peer},
-            device_id_type=pl.DeviceIdType.MESH,
-        )
-
-    def recv_wait(j, send_ref, recv_ref, send_sem, recv_sem):
-        pltpu.make_async_remote_copy(
-            src_ref=send_ref.at[0],
-            dst_ref=recv_ref.at[j],
-            send_sem=send_sem.at[0],
-            recv_sem=recv_sem.at[j],
-            device_id={"tp": tp},
-            device_id_type=pl.DeviceIdType.MESH,
-        ).wait_recv()
-
-    group = lax.div(tp * HEAD, 256)
-    window = jnp.left_shift(jnp.int32(2), group)
-
-    def pooled_of(c):
-        x = p_ref[c * CHUNK : (c + 1) * CHUNK + HALO, :]
-        s = x + pltpu.roll(x, 1, 0)
-        for level in (1, 2, 3):
-            s = jnp.where(group >= level, s + pltpu.roll(s, 2**level, 0), s)
-        s = s[HALO:, :]
-        x = x[HALO:, :]
-        at = lax.broadcasted_iota(jnp.int32, (HALO, HEAD), 0) + (sp * rows + c * CHUNK + 1)
-        count = jnp.minimum(at, window).astype(F32)
-        whole = jnp.minimum(lax.broadcasted_iota(jnp.int32, (1, HEAD), 1) + 4096, window).astype(F32)
-        top = s[:HALO, :] / count
-        rest = s[HALO:, :] * (1.0 / whole)
-        return (jnp.concatenate([top, rest], axis=0) - x).astype(BF16)
-
-    p_args = (psend_ref, prow_ref, psend_sem, precv_sem)
-    g_args = (gsend_ref, grow_ref, gsend_sem, grecv_sem)
-
-    def p_of(c):
-        return dot(x_ref[chunk_of(c), :], wp_ref[...])
-
-    p = p_of(0)
-    for c in range(n_ch):
+    p = p_of(EARLY)
+    for c in range(EARLY, n_ch):
         if c + 1 < n_ch:
             p_next = p_of(c + 1)
-        p_ref[HALO + c * CHUNK : HALO + (c + 1) * CHUNK, :] = p.astype(BF16).astype(F32)
-        decay_of_chunk(c)
-        if c > 0:
-            psend_ref[c] = pooled_of(c)
+        keep_p(c, p)
+        for d in range(2 * (c - EARLY), min(n_ch, 2 * (c - EARLY) + 2)):
+            decay_of_chunk(d)
+        if c == EARLY + 1:
+            send_pooled(*range(3, EARLY + 2))
         p = p_next
-
-    @pl.when(sp > 0)
-    def _():
-        halo_copy.wait_recv()
-        p_ref[0:HALO, :] = halo_ref[...].astype(F32)
-
-    @pl.when(sp == 0)
-    def _():
-        p_ref[0:HALO, :] = jnp.zeros((HALO, HEAD), F32)
-
-    psend_ref[0] = pooled_of(0)
-    for k in range(n_tp - 1):
-        row_copy(peer_of(*order[k]), *p_args).start()
-    prow_ref[tp] = psend_ref[tp]
+    send_pooled(*range(EARLY + 2, n_ch))
 
     w_copies[3].wait()
     w_copies[4].wait()
-    def keep_q(c, qg):
+    def mix(c, qg):
         here = chunk_of(c)
-        query = qg[:, :HEAD].astype(BF16).astype(F32)
-        g_ref[here, :] = qg[:, HEAD:].astype(BF16)
-        q_rot = turned(query, c).astype(BF16)
+        gate = qg[:, HEAD:]
+        g_ref[here, :] = (gate * jax.nn.sigmoid(gate)).astype(BF16)
+        q_rot = turned(qg[:, :HEAD], c).astype(BF16)
         q_ref[here, :] = q_rot
-        scores = dot_nt(q_rot, k_ref[here, :])
-        mixing = (scores * d_ref[c]).astype(BF16)
+        return (dot_nt(q_rot, k_ref[here, :]) * d_ref[c]).astype(BF16)
+
+    def retain(c, mixing):
+        here = chunk_of(c)
         inner = dot(mixing, v_ref[here, :])
-        cross = dot(q_rot, sloc_ref[c]) * ecol_ref[here, :]
-        acc_ref[here, :] = inner + cross
+        acc_ref[here, :] = inner + dot(q_ref[here, :], sloc_ref[c]) * ecol_ref[here, :]
 
     def row_states():
         for j in range(1, n_y):
@@ -431,14 +485,20 @@
                 for copy in column_sends(j):
                     copy.start()
 
-    qg = dot(x_ref[chunk_of(0), :], wqg_ref[...])
+    qg = dot(x_ref[x_rows(0), :], wqg_ref[...])
+    mixing = None
     for c in range(n_ch):
         if c + 1 < n_ch:
-            qg_next = dot(x_ref[chunk_of(c + 1), :], wqg_ref[...])
-        keep_q(c, qg)
-        qg = qg_next
+            qg_next = dot(x_ref[x_rows(c + 1), :], wqg_ref[...])
+        mixing_next = mix(c, qg)
+        if c > 0:
+            retain(c - 1, mixing)
+        qg, mixing = qg_next, mixing_next
         if c == ROW_AT:
             row_states()
+        if c == HALO_AT:
+            first_chunk()
+    retain(n_ch - 1, mixing)
 
     inc_ref[...] = jnp.zeros_like(inc_ref)
 
@@ -453,20 +513,27 @@
 
     small[3].wait()
 
-    def gated_of(c):
+    def cross_of(c):
+        return dot(q_ref[chunk_of(c), :], incoming)
+
+    def gated_of(c, cross):
         here = chunk_of(c)
-        cross = dot(q_ref[here, :], incoming) * (ecol_ref[here, :] * pre_ref[pl.ds(c, 1), :])
-        retained = acc_ref[here, :] + cross
+        retained = acc_ref[here, :] + cross * edev_ref[here, :]
         centered = retained - jnp.mean(retained, axis=-1, keepdims=True)
         scale = lax.rsqrt(jnp.mean(centered * centered, axis=-1, keepdims=True) + 1e-06)
-        gate = g_ref[here, :].astype(F32)
-        return (gate * jax.nn.sigmoid(gate) * gain_ref[...] * (centered * scale)).astype(BF16)
-
-    for k in range(n_tp - 1):
-        peer = peer_of(*order[k])
-        gsend_ref[peer] = gated_of(peer)
-        row_copy(peer, *g_args).start()
-    grow_ref[tp] = gated_of(tp)
+        return (g_ref[here, :].astype(F32) * gain_ref[...] * (centered * scale)).astype(BF16)
+
+    cross = cross_of(peers[0])
+    for k, peer in enumerate(peers):
+        if k + 1 < n_tp:
+            cross_next = cross_of(peers[k + 1])
+        chunk = gated_of(peer, cross)
+        if k + 1 < n_tp:
+            gsend_ref[peer] = chunk
+            row_copy(peer, *g_args).start()
+        else:
+            grow_ref[tp] = chunk
+        cross = cross_next
 
     wout_copy.wait()
     for j in range(n_tp):
@@ -535,7 +602,7 @@
         in_specs=[any_spec] * 11,
         out_specs=pl.BlockSpec(memory_space=pltpu.VMEM),
         scratch_shapes=[
-            vm((rows, depth), BF16),
+            vm((HALO + rows, depth), BF16),
             vm((depth, 2 * HEAD), BF16),
             vm((depth, 2 * HEAD), BF16),
             vm((depth, HEAD), BF16),
@@ -546,14 +613,20 @@
             vm((2, n_ch, HEAD), F32),
             vm((rows, HEAD), BF16),
             vm((rows, HEAD), BF16),
+            vm((n_ch, HEAD, CHUNK), BF16),
             vm((rows, HEAD), BF16),
             vm((rows, HEAD), BF16),
-            vm((rows + HALO, HEAD), F32),
+            vm((PAD + HALO + rows, HEAD), F32),
             vm((HALO, HEAD), BF16),
             vm((HALO, HEAD), BF16),
             vm((rows, HEAD), F32),
             vm((rows // HEAD, HEAD), F32),
             vm((HEAD, rows // HEAD), F32),
+            vm((rows, HEAD), F32),
+            vm((rows, HEAD), F32),
+            vm((rows, HEAD), F32),
+            vm((PAD + HALO + CHUNK, HEAD), F32),
+            vm((rows, HEAD), F32),
             vm((rows, HEAD), F32),
             vm((n_ch, CHUNK, CHUNK), F32),
             vm((n_ch, HEAD), F32),

time: 27.9 us -> 26.7 us (0.957)
  Pallas kernels: 26.8 us -> 25.6 us
    pallas_call x1, Pallas kernels: 26.8 us -> 25.6 us  [local(): pl.pallas_call(functools.partial(kernel, n_sp, n_tp), out_shape=pltpu.VME...]
where the time goes in v4:
time: 26.7 us; the launch traced here: 26.6 us
  Pallas kernels  25.6 us (96%)
  local copies, waits for them, and re-layouts  0.97 us (4%)
    pallas_call x1, Pallas kernels, local(): pl.pallas_call(functools.partial(kernel, n_sp, n_tp), out_shape=pltpu.VME...  25.6 us
    unnamed x1, local copies, waits for them, and re-layouts  0.97 us

profile of v4, /device:TPU:1, one launch (start us, length us, event | category | flops | bytes accessed | tf_op | source)
XLA Modules:
  0.0 26.6 jit_solution(17370681384187140254)
XLA Ops:
  0.0 25.6 %layer.1 = bf16[256,2048]{1,0:T(8,128)(2,1)S(1)} custom-call(bf16[2048,2048]{1,0:T(8,128)(2,1)} %tok_hbm.1, bf16[2048,128]{1,0:T(8,128)(2,1)} %wq_hbm.1, bf16[2048,128]{1,0:T(8,128)(2,1)} %wk_hbm.1, bf16[2048,128]{1,0:T(8,128)(2,1)} %wv_hbm.1, bf16[2048,128]{1,0:T(8,128)(2,1)} %wg_hbm.1, bf16[2048,128]{1,0:T(8,128)(2,1)} %wp_hbm.1, f32[1,128]{1,0:T(1,128)} %bitcast.3, ...), custom_call_target="tpu_custom_call" | custom-call | tf_op jit(solution)/shard_map/layer/pallas_call | solution.py:599
  25.6 1.0 %copy.13 = bf16[256,2048]{1,0:T(8,128)(2,1)} copy(bf16[256,2048]{1,0:T(8,128)(2,1)S(1)} %layer.1) | data formatting | bytes 2097152

commit v5 on v4

--- a/solution.py
+++ b/solution.py
@@ -428,7 +428,7 @@
     def _():
         halo_copy.start()
 
-    for j in (2, 1, 3):
+    for j in (3, 1, 2):
         for copy in row_sends(j):
             copy.start()
 
@@ -495,7 +495,17 @@
             retain(c - 1, mixing)
         qg, mixing = qg_next, mixing_next
         if c == ROW_AT:
-            row_states()
+
+            @pl.when(y != 0)
+            def _():
+                row_states()
+
+        if c == ROW_AT + 2:
+
+            @pl.when(y == 0)
+            def _():
+                row_states()
+
         if c == HALO_AT:
             first_chunk()
     retain(n_ch - 1, mixing)

time: 26.7 us -> 26.4 us (0.989)
  Pallas kernels: 25.6 us -> 25.2 us
    pallas_call x1, Pallas kernels: 25.6 us -> 25.2 us  [local(): pl.pallas_call(functools.partial(kernel, n_sp, n_tp), out_shape=pltpu.VME...]
where the time goes in v5:
time: 26.4 us; the launch traced here: 26.2 us
  Pallas kernels  25.2 us (95%)
  local copies, waits for them, and re-layouts  0.97 us (4%)
    pallas_call x1, Pallas kernels, local(): pl.pallas_call(functools.partial(kernel, n_sp, n_tp), out_shape=pltpu.VME...  25.2 us
    unnamed x1, local copies, waits for them, and re-layouts  0.97 us

profile of v5, /device:TPU:1, one launch (start us, length us, event | category | flops | bytes accessed | tf_op | source)
XLA Modules:
  0.0 26.2 jit_solution(5172444373884819705)
XLA Ops:
  0.0 25.2 %layer.1 = bf16[256,2048]{1,0:T(8,128)(2,1)S(1)} custom-call(bf16[2048,2048]{1,0:T(8,128)(2,1)} %tok_hbm.1, bf16[2048,128]{1,0:T(8,128)(2,1)} %wq_hbm.1, bf16[2048,128]{1,0:T(8,128)(2,1)} %wk_hbm.1, bf16[2048,128]{1,0:T(8,128)(2,1)} %wv_hbm.1, bf16[2048,128]{1,0:T(8,128)(2,1)} %wg_hbm.1, bf16[2048,128]{1,0:T(8,128)(2,1)} %wp_hbm.1, f32[1,128]{1,0:T(1,128)} %bitcast.3, ...), custom_call_target="tpu_custom_call" | custom-call | tf_op jit(solution)/shard_map/layer/pallas_call | solution.py:609
  25.2 1.0 %copy.13 = bf16[256,2048]{1,0:T(8,128)(2,1)} copy(bf16[256,2048]{1,0:T(8,128)(2,1)S(1)} %layer.1) | data formatting | bytes 2097152
